TPU v7x, 32 devices: a whole 2x2x4 slice. The times are simulated.
32 devices in a mesh: fs: 16 (over z, y, core), tp: 2 (over x).
Axes of the slice: x: 2, y: 2, z: 4, core: 2. Of those that a mesh axis runs over, the one named last changes fastest.
Arguments:
- tokens: bfloat16 [16384, 2048], P(('fs', 'tp')), may hold values from -8 to 8
- pre_mix_gain: float32 [2048], replicated, may hold values from 0.1 to 1.9
- post_mix_gain: float32 [2048], replicated, may hold values from 0.1 to 1.9
- pre_ffn_gain: float32 [2048], replicated, may hold values from 0.1 to 1.9
- post_ffn_gain: float32 [2048], replicated, may hold values from 0.1 to 1.9
- w_branch: bfloat16 [2048, 1024], P('fs', 'tp'), may hold values from -0.125 to 0.125
- w_gelu: bfloat16 [2048, 1024], P('fs', 'tp'), may hold values from -0.125 to 0.125
- conv_weight: bfloat16 [4, 1024], P(None, 'tp'), may hold values from -3 to 3
- w_rec: bfloat16 [2, 8, 128, 128], P(None, 'tp'), may hold values from -0.5 to 0.5
- w_inp: bfloat16 [2, 8, 128, 128], P(None, 'tp'), may hold values from -0.5 to 0.5
- decay: float32 [2, 1024], P(None, 'tp'), may hold values from 3 to 10
- out_weight_t: bfloat16 [2048, 1024], P('fs', 'tp'), may hold values from -0.1875 to 0.1875
- w_gate: bfloat16 [2048, 3072], P('fs', 'tp'), may hold values from -0.125 to 0.125
- w_up: bfloat16 [2048, 3072], P('fs', 'tp'), may hold values from -0.125 to 0.125
- down_weight_t: bfloat16 [2048, 3072], P('fs', 'tp'), may hold values from -0.109375 to 0.109375
Outputs:
- layer_out: bfloat16 [16384, 2048], P(('fs', 'tp'))
All inputs are finite; a program needn't handle non-finite values.
Results may differ from a plain program's by a relative error of at most 0.014.
Values may be sent and summed in bfloat16 or wider, within the bound.
No kernel may reach another device: no remote copies, remote signals or barrier semaphores. Data moves between devices by JAX's collectives and lax.ppermute only.
A program may use at most 128 MiB of HBM per device.

v0:
```python
import jax
import jax.numpy as jnp
from jax import lax
from jax.sharding import PartitionSpec as P

EPS = 1e-06


def normed(values, gain):
    factor = lax.rsqrt(jnp.mean(values * values, axis=-1, keepdims=True) + EPS)
    return values * factor * gain


def conv_short(branch, conv_weight):
    length = branch.shape[0]
    padded = jnp.pad(branch.astype(jnp.float32), ((2, 1), (0, 0)))
    weights = conv_weight.astype(jnp.float32)
    summed = weights[0] * padded[0:length]
    for offset in range(1, 4):
        summed = summed + weights[offset] * padded[offset : offset + length]
    return summed.astype(jnp.bfloat16)


def combine(earlier, later):
    return (earlier[0] * later[0], later[0] * earlier[1] + later[1])


def recurrence(conv_out, w_rec, w_inp, decay):
    length, channels = conv_out.shape
    blocks = w_rec.shape[0]
    grouped = conv_out.reshape(length, blocks, channels // blocks)
    rate_gate = jax.nn.sigmoid(
        jnp.einsum("lnc,ncd->lnd", grouped, w_rec, preferred_element_type=jnp.float32).reshape(
            length, channels
        )
    )
    inflow = jax.nn.sigmoid(
        jnp.einsum("lnc,ncd->lnd", grouped, w_inp, preferred_element_type=jnp.float32).reshape(
            length, channels
        )
    )
    log_retain = -8.0 * rate_gate * jax.nn.softplus(-decay)
    retain = jnp.exp(log_retain)
    feed = jnp.sqrt(-jnp.expm1(2.0 * log_retain)) * inflow * conv_out.astype(jnp.float32)
    unused_decay, states = lax.associative_scan(combine, (retain, feed), axis=0)
    return states


def gathered_product(normed_rows, left_weight, right_weight):
    row_piece = lax.all_gather(normed_rows, "tp", axis=0, tiled=True)
    return jnp.concatenate(
        [
            jnp.dot(row_piece, left_weight, preferred_element_type=jnp.float32),
            jnp.dot(row_piece, right_weight, preferred_element_type=jnp.float32),
        ],
        axis=1,
    )


def summed_rows(hidden, weight_t):
    return lax.psum_scatter(
        lax.dot_general(
            hidden, weight_t, (((1,), (1,)), ((), ())), preferred_element_type=jnp.float32
        ).astype(jnp.bfloat16),
        "tp",
        scatter_dimension=0,
        tiled=True,
    ).astype(jnp.float32)


def per_device(
    tokens,
    pre_mix_gain,
    post_mix_gain,
    pre_ffn_gain,
    post_ffn_gain,
    w_branch,
    w_gelu,
    conv_weight,
    w_rec,
    w_inp,
    decay,
    out_weight_t,
    w_gate,
    w_up,
    down_weight_t,
):
    branch_all, gelu_all, out_rows = (
        lax.all_gather(w_branch, "fs", axis=0, tiled=True),
        lax.all_gather(w_gelu, "fs", axis=0, tiled=True),
        lax.all_gather(out_weight_t, "fs", axis=0, tiled=True),
    )
    out_whole = lax.all_gather(out_rows, "tp", axis=1, tiled=True)
    stream = tokens.astype(jnp.float32)
    normed_in = normed(stream, pre_mix_gain).astype(jnp.bfloat16)
    both_in = gathered_product(normed_in, branch_all, gelu_all)
    channels = branch_all.shape[1]
    branch_in = both_in[:, :channels].astype(jnp.bfloat16)
    gelu_in = both_in[:, channels:].astype(jnp.bfloat16)
    conv_out = conv_short(branch_in, conv_weight)
    forward = recurrence(conv_out, w_rec[0], w_inp[0], decay[0])
    backward = jnp.flip(recurrence(jnp.flip(conv_out, 0), w_rec[1], w_inp[1], decay[1]), 0)
    mixer_hidden = (jax.nn.gelu(gelu_in.astype(jnp.float32)) * (forward + backward)).astype(
        jnp.bfloat16
    )
    own_hidden = lax.all_to_all(mixer_hidden, "tp", split_axis=0, concat_axis=1, tiled=True)
    mixer_sum = lax.dot_general(
        own_hidden, out_whole, (((1,), (1,)), ((), ())), preferred_element_type=jnp.float32
    )
    residual = (stream + normed(mixer_sum, post_mix_gain)).astype(jnp.bfloat16)
    middle = residual.astype(jnp.float32)
    normed_mid = normed(middle, pre_ffn_gain).astype(jnp.bfloat16)
    gate_all, up_all, down_all = (
        lax.all_gather(w_gate, "fs", axis=0, tiled=True),
        lax.all_gather(w_up, "fs", axis=0, tiled=True),
        lax.all_gather(down_weight_t, "fs", axis=0, tiled=True),
    )
    both_mid = gathered_product(normed_mid, gate_all, up_all)
    hidden_units = gate_all.shape[1]
    gate_proj = both_mid[:, :hidden_units]
    up_proj = both_mid[:, hidden_units:]
    ffn_hidden = (jax.nn.silu(gate_proj) * up_proj).astype(jnp.bfloat16)
    ffn_sum = summed_rows(ffn_hidden, down_all)
    return (middle + normed(ffn_sum, post_ffn_gain)).astype(jnp.bfloat16)


def solution(mesh):
    return jax.shard_map(
        per_device,
        mesh=mesh,
        in_specs=(
            P(("fs", "tp"), None),
            P(),
            P(),
            P(),
            P(),
            P("fs", "tp"),
            P("fs", "tp"),
            P(None, "tp"),
            P(None, "tp", None, None),
            P(None, "tp", None, None),
            P(None, "tp"),
            P("fs", "tp"),
            P("fs", "tp"),
            P("fs", "tp"),
            P("fs", "tp"),
        ),
        out_specs=P(("fs", "tp"), None),
        check_vma=False,
    )
```

profile of v0, /device:TPU:0, one launch (start us, length us, event | category | flops | bytes accessed | tf_op | source)
XLA Modules:
  0.0 898.2 jit_solution(10344242694818016376)
XLA Ops:
  12.7 41.0 %all-gather.16.cloned.1.call-done = bf16[2048,512]{1,0:T(8,128)(2,1)} async-done(((bf16[128,512]{1,0:T(8,128)(2,1)}), bf16[2048,512]{1,0:T(8,128)(2,1)}) %all-gather.16.cloned.1.call-update) | async-done | bytes 2097168 | tf_op jit(solution)/shard_map/all_gather | solution.py:91
  55.0 41.1 %all-gather.14.cloned.1.call-done = bf16[2048,512]{1,0:T(8,128)(2,1)} async-done(((bf16[128,512]{1,0:T(8,128)(2,1)}), bf16[2048,512]{1,0:T(8,128)(2,1)}) %all-gather.14.cloned.1.call-update) | async-done | bytes 2097168 | tf_op jit(solution)/shard_map/all_gather | solution.py:89
  96.1 57.0 %all-gather.10.cloned.1.call-done = bf16[1024,2048]{1,0:T(8,128)(2,1)} async-done(((bf16[512,2048]{1,0:T(8,128)(2,1)}), bf16[1024,2048]{1,0:T(8,128)(2,1)}) %all-gather.10.cloned.1.call-update) | async-done | bytes 4194320 | tf_op jit(solution)/shard_map/all_gather | solution.py:50
  153.1 5.2 fusion.18
  170.1 9.1 %multiply_exponential_fusion.1 = (f32[1024,512]{1,0:T(8,128)}, f32[1024,512]{1,0:T(8,128)}) fusion(f32[1024,512]{1,0:T(8,128)} %copy.41, f32[512]{0:T(512)S(1)} %bitcast.96, f32[1024,512]{1,0:T(8,128)} %copy.42, f32[512]{0:T(512)S(1)} %bitcast.93, f32[1024,512]{1,0:T(8,128)} %copy-done.1, f32[512]{0:T(512)S(1)} %bitcast.90, f32[512]{0:T(512)S(1)} %bitcast.87, ...), kind=kLoop, calls=%fused_computation.42 | loop fusion | flops 7340032 | bytes 10496000 | tf_op jit(solution)/shard_map/exp | solution.py:43
  179.2 6.3 slice.515
  185.6 6.3 slice.516
  191.8 6.3 slice.514
  198.1 6.2 slice.518
  204.3 4.3 fusion.60
  212.7 3.6 slice.520
  216.4 3.6 slice.524
  264.8 5.8 add_convert_fusion
  270.5 15.5 %rev.8 = bf16[1024,512]{1,0:T(8,128)(2,1)} reverse(bf16[1024,512]{1,0:T(8,128)(2,1)} %add_convert_fusion), dimensions={0} | reverse | bytes 2097152 | tf_op jit(solution)/shard_map/jit(_flip)/rev | solution.py:102
  297.5 6.2 multiply_exponential_fusion
  303.7 6.2 slice.593
  309.9 6.3 slice.594
  316.2 6.2 slice.592
  322.4 6.3 slice.596
  328.7 4.1 fusion.61
  332.8 3.6 slice.599
  336.4 3.6 slice.600
  340.1 3.7 slice.598
  343.7 3.8 slice.602
  416.8 3.7 slice.519
  421.1 6.3 slice.586
  427.4 6.4 slice.513
  475.4 3.7 slice.597
  479.8 6.3 slice.664
  486.1 6.4 slice.591
  507.6 4.6 pad.144
  514.6 8.8 pad.146
  525.8 4.9 pad.145
  547.4 4.6 pad.164
  554.4 8.6 pad.166
  565.5 4.7 pad.165
  570.2 4.0 add.428
  574.2 16.9 %rev.9 = f32[1024,512]{1,0:T(8,128)} reverse(f32[1024,512]{1,0:T(8,128)} %add.428), dimensions={0} | reverse | bytes 4194304 | tf_op jit(solution)/shard_map/jit(_flip)/rev | solution.py:102
  591.1 8.5 fusion.16
  601.2 17.0 %all_to_all.19 = bf16[2,512,512]{1,2,0:T(8,128)(2,1)} all-to-all(bf16[2,512,512]{1,2,0:T(8,128)(2,1)S(1)} %copy.40), channel_id=1, replica_groups=mesh['fs'=16,'tp'=2] {'tp'}, dimensions={0} | all-to-all | bytes 2097152 | tf_op jit(solution)/shard_map/all_to_all | solution.py:106
  618.1 5.0 multiply_reduce_fusion
  629.1 55.4 %all-gather.20.cloned.1.call-done = bf16[1024,2048]{1,0:T(8,128)(2,1)} async-done(((bf16[512,2048]{1,0:T(8,128)(2,1)}), bf16[1024,2048]{1,0:T(8,128)(2,1)}) %all-gather.20.cloned.1.call-update) | async-done | bytes 4194320 | tf_op jit(solution)/shard_map/all_gather | solution.py:50
  684.5 12.0 %fusion.81 = f32[1024,1536]{1,0:T(8,128)} fusion(bf16[1024,2048]{1,0:T(8,128)(2,1)} %all-gather.20.cloned.1.call-done, bf16[2048,1536]{1,0:T(8,128)(2,1)} %all-gather.22.cloned.1.call-done), kind=kOutput, calls=%fused_computation.177 | convolution fusion | flops 6442450944 | bytes 16777216 | tf_op jit(solution)/shard_map/dot_general | solution.py:53
  696.5 51.7 %all-gather.24.cloned.1.call-done = bf16[2048,1536]{1,0:T(8,128)(2,1)} async-done(((bf16[128,1536]{1,0:T(8,128)(2,1)}), bf16[2048,1536]{1,0:T(8,128)(2,1)}) %all-gather.24.cloned.1.call-update) | async-done | bytes 6291472 | tf_op jit(solution)/shard_map/all_gather | solution.py:115
  748.2 62.4 %all-gather.26.cloned.1.call-done = bf16[2048,1536]{1,0:T(8,128)(2,1)} async-done(((bf16[128,1536]{1,0:T(8,128)(2,1)}), bf16[2048,1536]{1,0:T(8,128)(2,1)}) %all-gather.26.cloned.1.call-update) | async-done | bytes 6291472 | tf_op jit(solution)/shard_map/all_gather | solution.py:116
  810.7 21.0 %convolution_convert_fusion = bf16[1024,2048]{1,0:T(8,128)(2,1)} fusion(bf16[2048,1536]{1,0:T(8,128)(2,1)} %all-gather.26.cloned.1.call-done, f32[1024,1536]{1,0:T(8,128)} %fusion.81, bf16[1024,2048]{1,0:T(8,128)(2,1)} %all-gather.20.cloned.1.call-done, bf16[2048,1536]{1,0:T(8,128)(2,1)} %all-gather.24.cloned.1.call-done), kind=kOutput, calls=%fused_computation.20 | convolution fusion | flops 12896436224 | bytes 27262976 | tf_op jit(solution)/shard_map/dot_general | solution.py:62
  831.7 53.2 %reduce-scatter.2.cloned.1.call-done = bf16[512,2048]{1,0:T(8,128)(2,1)} async-done(((bf16[1024,2048]{1,0:T(8,128)(2,1)}), bf16[512,2048]{1,0:T(8,128)(2,1)}) %reduce-scatter.2.cloned.1.call-update) | async-done | bytes 2097168 | tf_op jit(solution)/shard_map/reduce_scatter | solution.py:61
  887.1 4.1 fusion.9
  (342 shorter events, 241.9 us)
Async XLA Ops:
  6.5 3.6 copy-start
  6.5 3.6 copy-start.29
  6.5 47.2 %all-gather.16.cloned.1.call-start = ((), (), s32[]{:S(2)}) async-start(), calls=%async_computation.5 | async-start | bytes 2228224 | tf_op jit(solution)/shard_map/all_gather | solution.py:91
  7.3 88.8 %all-gather.14.cloned.1.call-start = ((), (), s32[]{:S(2)}) async-start(), calls=%async_computation.4 | async-start | bytes 2228224 | tf_op jit(solution)/shard_map/all_gather | solution.py:89
  8.0 145.1 %all-gather.10.cloned.1.call-start = ((), (), s32[]{:S(2)}) async-start(), calls=%async_computation.2 | async-start | bytes 6291456 | tf_op jit(solution)/shard_map/all_gather | solution.py:50
  12.0 42.3 %copy-start.25 = (bf16[4,512]{1,0:T(4,128)(2,1)S(1)}, bf16[4,512]{1,0:T(4,128)(2,1)}, u32[]{:S(2)}) copy-start(bf16[4,512]{1,0:T(4,128)(2,1)} %param.22) | copy-start | bytes 12292
  12.0 42.4 %copy-start.44 = (f32[2,512]{1,0:T(2,128)S(1)}, f32[2,512]{1,0:T(2,128)}, u32[]{:S(2)}) copy-start(f32[2,512]{1,0:T(2,128)} %param.25) | copy-start | bytes 12292
  12.1 579.1 %all-gather.12.cloned.1.call-start = ((), (), s32[]{:S(2)}) async-start(), calls=%async_computation.3 | async-start | bytes 2228224 | tf_op jit(solution)/shard_map/all_gather | solution.py:90
  12.6 605.5 %all-gather.18.cloned.1.call-start = ((), (), s32[]{:S(2)}) async-start(), calls=%async_computation.6 | async-start | bytes 6291456 | tf_op jit(solution)/shard_map/all_gather | solution.py:93
  53.7 575.4 %all-gather.22.cloned.1.call-start = ((), (), s32[]{:S(2)}) async-start(), calls=%async_computation.8 | async-start | bytes 6684672 | tf_op jit(solution)/shard_map/all_gather | solution.py:114
  54.3 630.2 %all-gather.20.cloned.1.call-start = ((), (), s32[]{:S(2)}) async-start(), calls=%async_computation.7 | async-start | bytes 6291456 | tf_op jit(solution)/shard_map/all_gather | solution.py:50
  54.4 115.7 %copy-start.18 = (f32[1,512]{1,0:T(1,128)}, f32[1,512]{1,0:T(1,128)S(1)}, u32[]{:S(2)}) copy-start(f32[1,512]{1,0:T(1,128)S(1)} %get-tuple-element.53) | copy-start | bytes 6148
  54.4 115.7 %copy-start.19 = (f32[1,512]{1,0:T(1,128)}, f32[1,512]{1,0:T(1,128)S(1)}, u32[]{:S(2)}) copy-start(f32[1,512]{1,0:T(1,128)S(1)} %get-tuple-element.54) | copy-start | bytes 6148
  54.4 115.7 %copy-start.20 = (f32[1,512]{1,0:T(1,128)}, f32[1,512]{1,0:T(1,128)S(1)}, u32[]{:S(2)}) copy-start(f32[1,512]{1,0:T(1,128)S(1)} %get-tuple-element.55) | copy-start | bytes 6148
  54.4 115.7 %copy-start.21 = (f32[1,512]{1,0:T(1,128)}, f32[1,512]{1,0:T(1,128)S(1)}, u32[]{:S(2)}) copy-start(f32[1,512]{1,0:T(1,128)S(1)} %get-tuple-element.56) | copy-start | bytes 6148
  161.5 3.4 copy-start.46
  286.1 3.4 copy-start.47
  421.1 42.9 %copy-start.7 = (f32[64,512]{1,0:T(8,128)S(1)}, f32[64,512]{1,0:T(8,128)}, u32[]{:S(2)}) copy-start(f32[64,512]{1,0:T(8,128)} %get-tuple-element.26) | copy-start | bytes 393220
  427.4 38.8 %copy-start.6 = (f32[128,512]{1,0:T(8,128)S(1)}, f32[128,512]{1,0:T(8,128)}, u32[]{:S(2)}) copy-start(f32[128,512]{1,0:T(8,128)} %get-tuple-element.22) | copy-start | bytes 786436
  427.4 45.9 %copy-start.4 = (f32[512,512]{1,0:T(8,128)S(1)}, f32[512,512]{1,0:T(8,128)}, u32[]{:S(2)}) copy-start(f32[512,512]{1,0:T(8,128)} %get-tuple-element.14) | copy-start | bytes 3145732
  479.6 14.1 %copy-start.24 = (f32[2,512]{1,0:T(2,128)S(1)}, f32[2,512]{1,0:T(2,128)}, u32[]{:S(2)}) copy-start(f32[2,512]{1,0:T(2,128)} %slice.562) | copy-start | bytes 12292
  479.7 14.1 %copy-start.26 = (f32[2,512]{1,0:T(2,128)S(1)}, f32[2,512]{1,0:T(2,128)}, u32[]{:S(2)}) copy-start(f32[2,512]{1,0:T(2,128)} %slice.563) | copy-start | bytes 12292
  479.7 14.1 %copy-start.27 = (f32[2,512]{1,0:T(2,128)S(1)}, f32[2,512]{1,0:T(2,128)}, u32[]{:S(2)}) copy-start(f32[2,512]{1,0:T(2,128)} %slice.564) | copy-start | bytes 12292
  479.7 14.2 %copy-start.28 = (f32[2,512]{1,0:T(2,128)S(1)}, f32[2,512]{1,0:T(2,128)}, u32[]{:S(2)}) copy-start(f32[2,512]{1,0:T(2,128)} %slice.566) | copy-start | bytes 12292
  479.7 14.2 %copy-start.17 = (f32[4,512]{1,0:T(4,128)S(1)}, f32[4,512]{1,0:T(4,128)}, u32[]{:S(2)}) copy-start(f32[4,512]{1,0:T(4,128)} %get-tuple-element.42) | copy-start | bytes 24580
  479.7 15.0 %copy-start.22 = (f32[3,512]{1,0:T(4,128)S(1)}, f32[3,512]{1,0:T(4,128)}, u32[]{:S(2)}) copy-start(f32[3,512]{1,0:T(4,128)} %slice.555) | copy-start | bytes 18436
  479.7 15.0 %copy-start.23 = (f32[3,512]{1,0:T(4,128)S(1)}, f32[3,512]{1,0:T(4,128)}, u32[]{:S(2)}) copy-start(f32[3,512]{1,0:T(4,128)} %slice.572) | copy-start | bytes 18436
  479.7 15.0 %copy-start.43 = (f32[1,512]{1,0:T(1,128)S(1)}, f32[1,512]{1,0:T(1,128)}, u32[]{:S(2)}) copy-start(f32[1,512]{1,0:T(1,128)} %slice.676) | copy-start | bytes 6148
  479.7 15.1 %copy-start.15 = (f32[7,512]{1,0:T(8,128)S(1)}, f32[7,512]{1,0:T(8,128)}, u32[]{:S(2)}) copy-start(f32[7,512]{1,0:T(8,128)} %slice.549) | copy-start | bytes 43012
  479.7 15.1 %copy-start.16 = (f32[7,512]{1,0:T(8,128)S(1)}, f32[7,512]{1,0:T(8,128)}, u32[]{:S(2)}) copy-start(f32[7,512]{1,0:T(8,128)} %slice.574) | copy-start | bytes 43012
  479.7 15.1 %copy-start.42 = (f32[1,512]{1,0:T(1,128)S(1)}, f32[1,512]{1,0:T(1,128)}, u32[]{:S(2)}) copy-start(f32[1,512]{1,0:T(1,128)} %slice.675) | copy-start | bytes 6148
  479.7 15.1 %copy-start.13 = (f32[15,512]{1,0:T(8,128)S(1)}, f32[15,512]{1,0:T(8,128)}, u32[]{:S(2)}) copy-start(f32[15,512]{1,0:T(8,128)} %slice.543) | copy-start | bytes 92164
  479.7 15.1 %copy-start.14 = (f32[15,512]{1,0:T(8,128)S(1)}, f32[15,512]{1,0:T(8,128)}, u32[]{:S(2)}) copy-start(f32[15,512]{1,0:T(8,128)} %slice.576) | copy-start | bytes 92164
  479.7 15.2 %copy-start.41 = (f32[1,512]{1,0:T(1,128)S(1)}, f32[1,512]{1,0:T(1,128)}, u32[]{:S(2)}) copy-start(f32[1,512]{1,0:T(1,128)} %slice.674) | copy-start | bytes 6148
  486.1 8.9 copy-start.11
  486.1 8.9 copy-start.12
  486.1 9.0 copy-start.40
  486.1 9.7 %copy-start.9 = (f32[63,512]{1,0:T(8,128)S(1)}, f32[63,512]{1,0:T(8,128)}, u32[]{:S(2)}) copy-start(f32[63,512]{1,0:T(8,128)} %slice.531) | copy-start | bytes 387076
  486.1 9.7 %copy-start.10 = (f32[63,512]{1,0:T(8,128)S(1)}, f32[63,512]{1,0:T(8,128)}, u32[]{:S(2)}) copy-start(f32[63,512]{1,0:T(8,128)} %slice.580) | copy-start | bytes 387076
  486.1 9.7 %copy-start.39 = (f32[1,512]{1,0:T(1,128)S(1)}, f32[1,512]{1,0:T(1,128)}, u32[]{:S(2)}) copy-start(f32[1,512]{1,0:T(1,128)} %slice.672) | copy-start | bytes 6148
  530.7 8.3 copy-start.8
  530.7 8.4 copy-start.36
  618.1 5.0 copy-start.30
  627.6 120.7 %all-gather.24.cloned.1.call-start = ((), (), s32[]{:S(2)}) async-start(), calls=%async_computation.9 | async-start | bytes 6684672 | tf_op jit(solution)/shard_map/all_gather | solution.py:115
  628.3 182.4 %all-gather.26.cloned.1.call-start = ((), (), s32[]{:S(2)}) async-start(), calls=%async_computation.10 | async-start | bytes 6684672 | tf_op jit(solution)/shard_map/all_gather | solution.py:116
  629.0 255.9 %reduce-scatter.2.cloned.1.call-start = ((), (), s32[]{:S(2)}) async-start(), calls=%async_computation.11 | async-start | bytes 6291456 | tf_op jit(solution)/shard_map/reduce_scatter | solution.py:61
  831.7 55.3 %copy-start.32 = (f32[2048]{0:T(1024)S(1)}, f32[2048]{0:T(1024)}, u32[]{:S(2)}) copy-start(f32[2048]{0:T(1024)} %param.19) | copy-start | bytes 24580
  831.7 55.3 %copy-start.3 = (bf16[512,2048]{1,0:T(8,128)(2,1)S(1)}, bf16[512,2048]{1,0:T(8,128)(2,1)}, u32[]{:S(2)}) copy-start(bf16[512,2048]{1,0:T(8,128)(2,1)} %copy-done.2) | copy-start | bytes 6291460
  (10 other events, 24.1 us)
Sparse Core Ops, SparseCore 0:
  9.5 44.1 all-gather.15
  55.9 40.1 all-gather.13
  97.6 55.4 all-gather.9
  155.1 41.4 all-gather.11
  198.0 55.4 all-gather.17
  255.6 61.3 all-gather.21
  627.7 56.7 all-gather.19
  686.8 61.3 all-gather.23
  750.5 60.0 all-gather.25
  831.8 53.0 reduce-scatter.1
where the time goes:
time: 914 us; the launch traced here: 898 us
  waiting for transfers between devices  366 us (40%)
  local copies, waits for them, and re-layouts  335 us (37%)
  other arithmetic  103 us (11%)
  matrix products  61.6 us (7%)
  blocking collectives  17 us (2%)
  between operations  14.8 us (2%)
    slice x120, local copies, waits for them, and re-layouts, recurrence(): unused_decay, states = lax.associative_scan(combine, (retain, feed), axis=0)  242 us
    all_gather x2, waiting for transfers between devices, gathered_product(): row_piece = lax.all_gather(normed_rows, 'tp', axis=0, tiled=True)  112 us
    all_gather x1, waiting for transfers between devices, per_device(): lax.all_gather(down_weight_t, 'fs', axis=0, tiled=True)  62.4 us
    reduce_scatter x1, waiting for transfers between devices, summed_rows(): lax.psum_scatter(lax.dot_general(hidden, weight_t, (((1,), (1,)), ((), ()...  53.2 us
    all_gather x1, waiting for transfers between devices, per_device(): lax.all_gather(w_up, 'fs', axis=0, tiled=True)  51.7 us
    pad x36, local copies, waits for them, and re-layouts, recurrence(): unused_decay, states = lax.associative_scan(combine, (retain, feed), axis=0)  44.9 us
    all_gather x1, waiting for transfers between devices, per_device(): lax.all_gather(w_branch, 'fs', axis=0, tiled=True)  41.1 us
    all_gather x1, waiting for transfers between devices, per_device(): lax.all_gather(out_weight_t, 'fs', axis=0, tiled=True)  41 us
  transfers between devices with their start and end apart: 10, of which 7 were waited for; matrix products, arithmetic and copies ran while one was open for 52% of the time, Pallas kernels for 0%

commit v1 on v0

v1 whole, which is shorter than its diff:
```python
import functools

import jax
import jax.numpy as jnp
from jax import lax
from jax.experimental import pallas as pl
from jax.experimental.pallas import tpu as pltpu
from jax.sharding import PartitionSpec as P

EPS = 1e-06
SEGMENTS = 8
LANES = 128
F32 = jnp.float32
BF16 = jnp.bfloat16


def normed(values, gain):
    factor = lax.rsqrt(jnp.mean(values * values, axis=-1, keepdims=True) + EPS)
    return values * factor * gain


def tile_of(size, limit):
    tile = min(size, limit)
    while size % tile:
        tile -= LANES
    return tile


def one_minus_exp(y):
    series = 1.0 + y * (1.0 / 6.0)
    for term in (5.0, 4.0, 3.0, 2.0):
        series = 1.0 + y * (1.0 / term) * series
    return jnp.where(y > -0.25, -y * series, 1.0 - jnp.exp(y))


def dot_nn(left, right):
    return jnp.dot(left, right, preferred_element_type=F32)


def dot_nt(left, right):
    return lax.dot_general(left, right, (((1,), (1,)), ((), ())), preferred_element_type=F32)


def mixer_kernel(
    place_ref, own_ref, other_ref, wb_ref, wg_ref, cw_ref, rec_ref, inp_ref, slope_ref,
    mine_ref, theirs_ref, branch_ref, gelu_ref, a0, b0, a1, b1, hf, hb,
):
    half = own_ref.shape[0]
    length = 2 * half
    steps = length // SEGMENTS
    blocks = rec_ref.shape[1]
    own_at = pl.multiple_of(place_ref[0] * half, half)
    other_at = pl.multiple_of((1 - place_ref[0]) * half, half)
    for source, start in ((own_ref, own_at), (other_ref, other_at)):
        rows = source[...]
        branch_ref[pl.ds(start, half), :] = dot_nn(rows, wb_ref[...]).astype(BF16).astype(F32)
        gelu_ref[pl.ds(start, half), :] = dot_nn(rows, wg_ref[...]).astype(BF16)
    row = lax.broadcasted_iota(jnp.int32, (length, LANES), 0)
    for block in range(blocks):
        cols = slice(block * LANES, (block + 1) * LANES)
        branch = branch_ref[:, cols]
        taps = cw_ref[:, cols].astype(F32)
        summed = taps[0:1] * jnp.where(row >= 2, pltpu.roll(branch, 2, 0), 0.0)
        summed = summed + taps[1:2] * jnp.where(row >= 1, pltpu.roll(branch, 1, 0), 0.0)
        summed = summed + taps[2:3] * branch
        summed = summed + taps[3:4] * jnp.where(
            row < length - 1, pltpu.roll(branch, length - 1, 0), 0.0
        )
        conv = summed.astype(BF16)
        conv_wide = conv.astype(F32)
        for direction, (a_ref, b_ref) in enumerate(((a0, b0), (a1, b1))):
            rate = jax.nn.sigmoid(dot_nn(conv, rec_ref[direction, block]))
            inflow = jax.nn.sigmoid(dot_nn(conv, inp_ref[direction, block]))
            log_a = rate * slope_ref[direction : direction + 1, cols]
            a_ref[block] = jnp.exp(log_a)
            b_ref[block] = jnp.sqrt(one_minus_exp(2.0 * log_a)) * inflow * conv_wide

    def at(step):
        return pl.ds(step, SEGMENTS, stride=steps)

    def advance(step, states, store):
        new = []
        back = steps - 1 - step
        for block in range(blocks):
            for ar, br, hr, where in ((a0, b0, hf, step), (a1, b1, hb, back)):
                state, product = states[len(new)]
                keep = ar[block, at(where), :]
                state = keep * state + br[block, at(where), :]
                if store:
                    hr[block, at(where), :] = state
                else:
                    product = product * keep
                new.append((state, product))
        return tuple(new)

    zero = jnp.zeros((SEGMENTS, LANES), F32)
    one = jnp.ones((SEGMENTS, LANES), F32)
    ends = lax.fori_loop(
        0, steps, lambda i, s: advance(i, s, False), ((zero, one),) * (2 * blocks), unroll=8
    )
    starts = []
    for index, (state, product) in enumerate(ends):
        order = list(range(SEGMENTS))
        if index % 2:
            order = order[::-1]
        rows = [None] * SEGMENTS
        carry = zero[0:1]
        for segment in order:
            rows[segment] = carry
            carry = state[segment : segment + 1] + product[segment : segment + 1] * carry
        starts.append((jnp.concatenate(rows, axis=0), zero))
    lax.fori_loop(0, steps, lambda i, s: advance(i, s, True), tuple(starts), unroll=8)
    for target, start in ((mine_ref, own_at), (theirs_ref, other_at)):
        for block in range(blocks):
            cols = slice(block * LANES, (block + 1) * LANES)
            states = hf[block, pl.ds(start, half), :] + hb[block, pl.ds(start, half), :]
            factor = jax.nn.gelu(gelu_ref[pl.ds(start, half), cols].astype(F32))
            target[:, cols] = (factor * states).astype(BF16)


def mixer(place, own, other, gathered, conv_weight, w_rec, w_inp, slope):
    half, width = own.shape
    channels = conv_weight.shape[1]
    group = tile_of(channels, 2 * LANES)
    blocks = group // LANES
    count = channels // group
    length = 2 * half
    wide = pltpu.VMEM((blocks, length, LANES), F32)
    whole = pl.BlockSpec((half, width), lambda j: (0, 0))
    maps = pl.BlockSpec((2, blocks, LANES, LANES), lambda j: (0, j, 0, 0))
    piece = pl.BlockSpec((half, group), lambda j: (0, j))
    return pl.pallas_call(
        mixer_kernel,
        grid=(count,),
        in_specs=[
            pl.BlockSpec(memory_space=pltpu.SMEM),
            whole,
            whole,
            pl.BlockSpec((width, group), lambda j: (0, j)),
            pl.BlockSpec((width, group), lambda j: (0, count + j)),
            pl.BlockSpec((conv_weight.shape[0], group), lambda j: (0, j)),
            maps,
            maps,
            pl.BlockSpec((2, group), lambda j: (0, j)),
        ],
        out_specs=[piece, piece],
        out_shape=[jax.ShapeDtypeStruct((half, channels), BF16)] * 2,
        scratch_shapes=[
            pltpu.VMEM((length, group), F32),
            pltpu.VMEM((length, group), BF16),
            wide, wide, wide, wide, wide, wide,
        ],
        compiler_params=pltpu.CompilerParams(vmem_limit_bytes=56 * 2**20),
        name="mixer",
    )(place, own, other, gathered, gathered, conv_weight, w_rec, w_inp, slope)


def out_kernel(ha_ref, hb_ref, wa_ref, wb_ref, tok_ref, gain_ref, mid_gain_ref, res_ref, mid_ref):
    summed = dot_nt(ha_ref[...], wa_ref[...]) + dot_nt(hb_ref[...], wb_ref[...])
    residual = (tok_ref[...].astype(F32) + normed(summed, gain_ref[...])).astype(BF16)
    res_ref[...] = residual
    mid_ref[...] = normed(residual.astype(F32), mid_gain_ref[...]).astype(BF16)


def out_projection(ha, hb, wa, wa_block, wb, wb_block, tokens, gain, mid_gain):
    rows, width = tokens.shape
    tile = min(rows, 256)
    channels = ha.shape[1]
    hidden = pl.BlockSpec((tile, channels), lambda i: (i, 0))
    wide = pl.BlockSpec((tile, width), lambda i: (i, 0))
    gains = pl.BlockSpec((1, width), lambda i: (0, 0))
    return pl.pallas_call(
        out_kernel,
        grid=(rows // tile,),
        in_specs=[
            hidden,
            hidden,
            pl.BlockSpec((width, channels), lambda i: (0, wa_block)),
            pl.BlockSpec((width, channels), lambda i: (0, wb_block)),
            wide,
            gains,
            gains,
        ],
        out_specs=[wide, wide],
        out_shape=[jax.ShapeDtypeStruct((rows, width), BF16)] * 2,
        compiler_params=pltpu.CompilerParams(vmem_limit_bytes=56 * 2**20),
        name="out_projection",
    )(ha, hb, wa, wb, tokens, gain[None], mid_gain[None])


def ffn_kernel(x_ref, gate_ref, up_ref, down_ref, out_ref, acc_ref):
    rows = x_ref[...]
    gate = dot_nn(rows, gate_ref[...])
    hidden = (gate * jax.nn.sigmoid(gate) * dot_nn(rows, up_ref[...])).astype(BF16)
    partial = dot_nt(hidden, down_ref[...])
    step = pl.program_id(0)
    last = pl.num_programs(0) - 1

    @pl.when(step == 0)
    def _():
        acc_ref[...] = partial

    @pl.when(step > 0)
    def _():
        acc_ref[...] += partial

    @pl.when(step == last)
    def _():
        out_ref[...] = acc_ref[...].astype(BF16)


def ffn(rows, gathered):
    count, width = rows.shape
    hidden_units = gathered.shape[1] // 3
    tile = tile_of(hidden_units, 512)
    tiles = hidden_units // tile
    whole = pl.BlockSpec((count, width), lambda j: (0, 0))
    return pl.pallas_call(
        ffn_kernel,
        grid=(tiles,),
        in_specs=[
            whole,
            pl.BlockSpec((width, tile), lambda j: (0, j)),
            pl.BlockSpec((width, tile), lambda j: (0, tiles + j)),
            pl.BlockSpec((width, tile), lambda j: (0, 2 * tiles + j)),
        ],
        out_specs=whole,
        out_shape=jax.ShapeDtypeStruct((count, width), BF16),
        scratch_shapes=[pltpu.VMEM((count, width), F32)],
        compiler_params=pltpu.CompilerParams(vmem_limit_bytes=56 * 2**20),
        name="ffn",
    )(rows, gathered, gathered, gathered)


def per_device(
    ranks,
    tokens,
    pre_mix_gain,
    post_mix_gain,
    pre_ffn_gain,
    post_ffn_gain,
    w_branch,
    w_gelu,
    conv_weight,
    w_rec,
    w_inp,
    decay,
    out_weight_t,
    w_gate,
    w_up,
    down_weight_t,
):
    swap = [(0, 1), (1, 0)]
    rows = tokens.shape[0]
    mix_shard = jnp.concatenate([w_branch, w_gelu, out_weight_t], axis=1)
    ffn_shard = jnp.concatenate([w_gate, w_up, down_weight_t], axis=1)
    mix_all = lax.all_gather(mix_shard, "fs", axis=0, tiled=True)
    mix_all, ffn_shard = lax.optimization_barrier((mix_all, ffn_shard))
    ffn_all = lax.all_gather(ffn_shard, "fs", axis=0, tiled=True)
    channels = w_branch.shape[1]
    stream = tokens.astype(F32)
    normed_in = normed(stream, pre_mix_gain).astype(BF16)
    slope = -8.0 * jax.nn.softplus(-decay)
    place = lax.axis_index("tp").astype(jnp.int32).reshape(1)
    if ranks == 2:
        other_in = lax.ppermute(normed_in, "tp", swap)
        out_other = lax.ppermute(mix_all[:, 2 * channels :], "tp", swap)
        mine, theirs = mixer(
            place, normed_in, other_in, mix_all, conv_weight, w_rec, w_inp, slope
        )
        received = lax.ppermute(theirs, "tp", swap)
        residual, normed_mid = out_projection(
            mine, received, mix_all, 2, out_other, 0, tokens, post_mix_gain, pre_ffn_gain
        )
        other_mid = lax.ppermute(normed_mid, "tp", swap)
        pieces = 2 if rows % 512 == 0 else 1
        size = rows // pieces
        returned = []
        for piece in range(pieces):
            part = ffn(lax.slice_in_dim(other_mid, piece * size, (piece + 1) * size), ffn_all)
            returned.append(lax.ppermute(part, "tp", swap))
        own_part = ffn(normed_mid, ffn_all)
        ffn_sum = own_part.astype(F32) + jnp.concatenate(returned, axis=0).astype(F32)
    else:
        everything = lax.all_gather(normed_in, "tp", axis=0, tiled=True)
        half = everything.shape[0] // 2
        first, second = mixer(
            place * 0, everything[:half], everything[half:], mix_all, conv_weight, w_rec, w_inp, slope
        )
        hidden = lax.all_to_all(
            jnp.concatenate([first, second], axis=0), "tp", split_axis=0, concat_axis=1, tiled=True
        )
        out_whole = lax.all_gather(mix_all[:, 2 * channels :], "tp", axis=1, tiled=True)
        mid_cols = hidden.shape[1] // 2
        residual, normed_mid = out_projection(
            hidden[:, :mid_cols], hidden[:, mid_cols:], out_whole, 0, out_whole, 1,
            tokens, post_mix_gain, pre_ffn_gain,
        )
        every_mid = lax.all_gather(normed_mid, "tp", axis=0, tiled=True)
        ffn_sum = lax.psum_scatter(
            ffn(every_mid, ffn_all), "tp", scatter_dimension=0, tiled=True
        ).astype(F32)
    return (residual.astype(F32) + normed(ffn_sum, post_ffn_gain)).astype(BF16)


def solution(mesh):
    return jax.shard_map(
        functools.partial(per_device, mesh.shape["tp"]),
        mesh=mesh,
        in_specs=(
            P(("fs", "tp"), None),
            P(),
            P(),
            P(),
            P(),
            P("fs", "tp"),
            P("fs", "tp"),
            P(None, "tp"),
            P(None, "tp", None, None),
            P(None, "tp", None, None),
            P(None, "tp"),
            P("fs", "tp"),
            P("fs", "tp"),
            P("fs", "tp"),
            P("fs", "tp"),
        ),
        out_specs=P(("fs", "tp"), None),
        check_vma=False,
    )
```

time: 914 us -> 308 us (0.34); the launches traced: 898 us -> 308 us
  local copies, waits for them, and re-layouts: 335 us -> 6.75 us
  waiting for transfers between devices: 366 us -> 190 us
  other arithmetic: 103 us -> 12.6 us
  Pallas kernels: 0 us -> 78.4 us
  matrix products: 61.6 us -> 0 us
  blocking collectives: 17 us -> 0 us
    all_gather x9 -> x2, waiting for transfers between devices: 309 us -> 62.8 us  [the longest x1 62.8 us: per_device(): mix_all = lax.all_gather(mix_shard, 'fs', axis=0, tiled=True)]
    slice x121 -> x2, local copies, waits for them, and re-layouts: 242 us -> 4.53 us  [the longest x1 3.06 us: per_device(): out_other = lax.ppermute(mix_all[:, 2 * channels:], 'tp', swap)]
    ppermute x0 -> x6, waiting for transfers between devices: none -> 127 us  [the longest x1 45.7 us: per_device(): other_mid = lax.ppermute(normed_mid, 'tp', swap)]
    pallas_call x0 -> x5, Pallas kernels: none -> 78.4 us  [the longest x3 40.7 us: ffn(): pl.pallas_call(ffn_kernel, grid=(tiles,), in_specs=[whole, pl.BlockSpec((...]
    dot_general x9 -> x0, matrix products: 61.6 us -> none  [the longest x1 21 us: summed_rows(): lax.dot_general(hidden, weight_t, (((1,), (1,)), ((), ())), preferred_ele...]
    reduce_scatter x1 -> x0, waiting for transfers between devices: 53.2 us -> none  [summed_rows(): lax.psum_scatter(lax.dot_general(hidden, weight_t, (((1,), (1,)), ((), ()...]
    pad x36 -> x0, local copies, waits for them, and re-layouts: 44.9 us -> none  [recurrence(): unused_decay, states = lax.associative_scan(combine, (retain, feed), axis=0)]
    mul x17 -> x1, other arithmetic: 33.5 us -> 0.61 us  [per_device(): slope = -8.0 * jax.nn.softplus(-decay)]
  transfers between devices with their start and end apart: 10 -> 8, of which waited for: 7 -> 5; matrix products, arithmetic and copies ran while one was open for 52% -> 3% of each run, Pallas kernels for 0% -> 22%
where the time goes in v1:
time: 308 us
  waiting for transfers between devices  190 us (62%)
  Pallas kernels  78.4 us (25%)
  between operations  13.5 us (4%)
  other arithmetic  12.6 us (4%)
  starting transfers between devices  7.02 us (2%)
  local copies, waits for them, and re-layouts  6.75 us (2%)
    all_gather x1, waiting for transfers between devices, per_device(): mix_all = lax.all_gather(mix_shard, 'fs', axis=0, tiled=True)  62.8 us
    ppermute x1, waiting for transfers between devices, per_device(): other_mid = lax.ppermute(normed_mid, 'tp', swap)  45.7 us
    ppermute x1, waiting for transfers between devices, per_device(): other_in = lax.ppermute(normed_in, 'tp', swap)  43 us
    pallas_call x3, Pallas kernels, ffn(): pl.pallas_call(ffn_kernel, grid=(tiles,), in_specs=[whole, pl.BlockSpec((...  40.7 us
    pallas_call x1, Pallas kernels, mixer(): pl.pallas_call(mixer_kernel, grid=(count,), in_specs=[pl.BlockSpec(memory...  29.8 us
    ppermute x1, waiting for transfers between devices, per_device(): received = lax.ppermute(theirs, 'tp', swap)  22.9 us
    ppermute x2, waiting for transfers between devices, per_device(): returned.append(lax.ppermute(part, 'tp', swap))  15.3 us
    pallas_call x1, Pallas kernels, out_projection(): pl.pallas_call(out_kernel, grid=(rows // tile,), in_specs=[hidden, hidden...  7.89 us
  transfers between devices with their start and end apart: 8, of which 5 were waited for; matrix products, arithmetic and copies ran while one was open for 3% of the time, Pallas kernels for 22%

profile of v1, /device:TPU:0, one launch (start us, length us, event | category | flops | bytes accessed | tf_op | source)
XLA Modules:
  0.0 308.0 jit_solution(6282179469262723383)
XLA Ops:
  6.5 0.0 copy-start
  6.5 0.0 all-gather.3.cloned.1.call-start
  6.5 1.9 pad_maximum_fusion.2
  8.5 0.0 all-gather.3.cloned.1.call-update
  8.5 0.0 copy-start.5
  8.5 0.0 all-gather.5.cloned.1.call-start
  8.6 2.4 pad_maximum_fusion.1
  10.9 62.8 %all-gather.3.cloned.1.call-done.wb_ref.wg_ref.wa_ref = bf16[2048,1536]{1,0:T(8,128)(2,1)} async-done(((bf16[128,1536]{1,0:T(8,128)(2,1)}), bf16[2048,1536]{1,0:T(8,128)(2,1)}) %all-gather.3.cloned.1.call-update) | async-done | bytes 6291472 | tf_op jit(solution)/shard_map/all_gather | solution.py:257
  73.8 0.0 all-gather.5.cloned.1.call-update
  73.8 0.0 copy-done
  73.8 0.5 fusion
  74.3 0.0 copy-done.5
  74.3 1.9 fusion.2.own_ref
  76.2 0.0 copy-start.7
  76.2 1.5 collective-permute-start
  77.6 3.1 slice.9
  80.7 0.6 collective-permute-start.2
  81.3 0.0 copy-done.7
  81.3 0.6 fusion.3.slope_ref
  81.9 43.0 %collective-permute-done.other_ref = bf16[512,2048]{1,0:T(8,128)(2,1)S(1)} collective-permute-done((bf16[512,2048]{1,0:T(8,128)(2,1)}, bf16[512,2048]{1,0:T(8,128)(2,1)S(1)}, u32[]{:S(2)}, u32[]{:S(2)}) %collective-permute-start) | collective-permute-done | bytes 2097184 | tf_op jit(solution)/shard_map/ppermute | solution.py:266
  124.9 0.0 copy-start.2
  124.9 1.4 copy-done.2
  126.2 29.8 %mixer.1 = (bf16[512,512]{1,0:T(8,128)(2,1)}, bf16[512,512]{1,0:T(8,128)(2,1)}) custom-call(s32[1]{0:T(128)} %bitcast.place_ref, bf16[512,2048]{1,0:T(8,128)(2,1)} %fusion.2.own_ref, bf16[512,2048]{1,0:T(8,128)(2,1)} %copy-done.2, bf16[2048,1536]{1,0:T(8,128)(2,1)} %all-gather.3.cloned.1.call-done.wb_ref.wg_ref.wa_ref, ...), custom_call_target="tpu_custom_call" | custom-call | tf_op jit(solution)/shard_map/mixer/pallas_call | solution.py:132
  156.0 1.5 collective-permute-start.1
  157.5 22.9 %collective-permute-done.1.hb_ref = bf16[512,512]{1,0:T(8,128)(2,1)S(1)} collective-permute-done((bf16[512,512]{1,0:T(8,128)(2,1)}, bf16[512,512]{1,0:T(8,128)(2,1)S(1)}, u32[]{:S(2)}, u32[]{:S(2)}) %collective-permute-start.1) | collective-permute-done | bytes 524320 | tf_op jit(solution)/shard_map/ppermute | solution.py:271
  180.3 0.0 copy-start.4
  180.3 0.0 collective-permute-done.2.wb_ref
  180.4 0.8 copy-done.4
  181.2 7.9 %out_projection.1 = (bf16[512,2048]{1,0:T(8,128)(2,1)}, bf16[512,2048]{1,0:T(8,128)(2,1)}) custom-call(bf16[512,512]{1,0:T(8,128)(2,1)} %get-tuple-element.12.ha_ref, bf16[512,512]{1,0:T(8,128)(2,1)} %copy-done.4, bf16[2048,1536]{1,0:T(8,128)(2,1)} %all-gather.3.cloned.1.call-done.wb_ref.wg_ref.wa_ref, bf16[2048,512]{1,0:T(8,128)(2,1)} %collective-permute-done.2.wb_ref, ...), custom_call_target="tpu_custom_call" | custom-call | tf_op jit(solution)/shard_map/out_projection/pallas_call | solution.py:172
  189.1 1.5 collective-permute-start.3
  190.6 45.7 %collective-permute-done.3 = bf16[512,2048]{1,0:T(8,128)(2,1)S(1)} collective-permute-done((bf16[512,2048]{1,0:T(8,128)(2,1)}, bf16[512,2048]{1,0:T(8,128)(2,1)S(1)}, u32[]{:S(2)}, u32[]{:S(2)}) %collective-permute-start.3) | collective-permute-done | bytes 2097184 | tf_op jit(solution)/shard_map/ppermute | solution.py:275
  236.2 1.5 fusion.4
  237.7 0.0 all-gather.5.cloned.1.call-done.gate_ref.up_ref.down_ref
  237.7 11.8 %ffn.4 = bf16[256,2048]{1,0:T(8,128)(2,1)} custom-call(bf16[256,2048]{1,0:T(8,128)(2,1)} %get-tuple-element.17.x_ref, bf16[2048,4608]{1,0:T(8,128)(2,1)} %all-gather.5.cloned.1.call-done.gate_ref.up_ref.down_ref, bf16[2048,4608]{1,0:T(8,128)(2,1)} %all-gather.5.cloned.1.call-done.gate_ref.up_ref.down_ref, ...), custom_call_target="tpu_custom_call" | custom-call | tf_op jit(solution)/shard_map/ffn/pallas_call | solution.py:218
  249.5 1.5 collective-permute-start.4
  251.0 11.8 %ffn.5 = bf16[256,2048]{1,0:T(8,128)(2,1)} custom-call(bf16[256,2048]{1,0:T(8,128)(2,1)} %get-tuple-element.18.x_ref, bf16[2048,4608]{1,0:T(8,128)(2,1)} %all-gather.5.cloned.1.call-done.gate_ref.up_ref.down_ref, bf16[2048,4608]{1,0:T(8,128)(2,1)} %all-gather.5.cloned.1.call-done.gate_ref.up_ref.down_ref, ...), custom_call_target="tpu_custom_call" | custom-call | tf_op jit(solution)/shard_map/ffn/pallas_call | solution.py:218
  262.8 0.6 collective-permute-start.5
  263.4 0.0 copy-start.6
  263.4 17.1 %ffn.3 = bf16[512,2048]{1,0:T(8,128)(2,1)} custom-call(bf16[512,2048]{1,0:T(8,128)(2,1)} %get-tuple-element.15.x_ref, bf16[2048,4608]{1,0:T(8,128)(2,1)} %all-gather.5.cloned.1.call-done.gate_ref.up_ref.down_ref, bf16[2048,4608]{1,0:T(8,128)(2,1)} %all-gather.5.cloned.1.call-done.gate_ref.up_ref.down_ref, ...), custom_call_target="tpu_custom_call" | custom-call | tf_op jit(solution)/shard_map/ffn/pallas_call | solution.py:218
  280.5 0.0 copy-start.1
  280.5 0.0 copy-start.3
  280.5 0.0 collective-permute-done.4
  280.5 15.3 %collective-permute-done.5 = bf16[256,2048]{1,0:T(8,128)(2,1)S(1)} collective-permute-done((bf16[256,2048]{1,0:T(8,128)(2,1)}, bf16[256,2048]{1,0:T(8,128)(2,1)S(1)}, u32[]{:S(2)}, u32[]{:S(2)}) %collective-permute-start.5) | collective-permute-done | bytes 1048608 | tf_op jit(solution)/shard_map/ppermute | solution.py:281
  295.8 2.3 multiply_reduce_fusion
  298.1 0.0 copy-done.6
  298.2 0.0 copy-done.1
  298.2 0.0 copy-done.3
  298.2 3.0 add_convert_fusion
  (2 shorter events, 0.0 us)
Async XLA Ops:
  6.5 67.3 %copy-start = (bf16[512,2048]{1,0:T(8,128)(2,1)S(1)}, bf16[512,2048]{1,0:T(8,128)(2,1)}, u32[]{:S(2)}) copy-start(bf16[512,2048]{1,0:T(8,128)(2,1)} %tok_ref.1) | copy-start | bytes 6291460
  6.5 67.2 %all-gather.3.cloned.1.call-start = ((), (), s32[]{:S(2)}) async-start(), calls=%async_computation | async-start | bytes 6684672 | tf_op jit(solution)/shard_map/all_gather | solution.py:257
  8.5 65.8 %copy-start.5 = (f32[2048]{0:T(1024)S(1)}, f32[2048]{0:T(1024)}, u32[]{:S(2)}) copy-start(f32[2048]{0:T(1024)} %param.16) | copy-start | bytes 24580
  8.5 229.2 %all-gather.5.cloned.1.call-start = ((), (), s32[]{:S(2)}) async-start(), calls=%async_computation.1 | async-start | bytes 20054016 | tf_op jit(solution)/shard_map/all_gather | solution.py:259
  76.2 5.1 %copy-start.7 = (f32[2,512]{1,0:T(2,128)S(1)}, f32[2,512]{1,0:T(2,128)}, u32[]{:S(2)}) copy-start(f32[2,512]{1,0:T(2,128)} %param.25) | copy-start | bytes 12292
  76.2 48.7 %collective-permute-start = (bf16[512,2048]{1,0:T(8,128)(2,1)}, bf16[512,2048]{1,0:T(8,128)(2,1)S(1)}, u32[]{:S(2)}, u32[]{:S(2)}) collective-permute-start(bf16[512,2048]{1,0:T(8,128)(2,1)} %fusion.2.own_ref), channel_id=1, source_target_pairs={{0,1},{1,0},{2,3},{3,2},{4,5},{5,4},{6,7},{7,6},{8,9},{9,8},{10,11... | collective-permute-start | bytes 6291464 | tf_op jit(solution)/shard_map/ppermute | solution.py:266
  80.7 99.7 %collective-permute-start.2 = (bf16[2048,512]{1,0:T(8,128)(2,1)}, bf16[2048,512]{1,0:T(8,128)(2,1)}, u32[]{:S(2)}, u32[]{:S(2)}) collective-permute-start(bf16[2048,512]{1,0:T(8,128)(2,1)} %slice.9), channel_id=1, source_target_pairs={{0,1},{1,0},{2,3},{3,2},{4,5},{5,4},{6,7},{7,6},{8,9},{9,8},{10,11... | collective-permute-start | bytes 6291464 | tf_op jit(solution)/shard_map/ppermute | solution.py:267
  124.9 1.4 copy-start.2
  156.0 24.3 %collective-permute-start.1 = (bf16[512,512]{1,0:T(8,128)(2,1)}, bf16[512,512]{1,0:T(8,128)(2,1)S(1)}, u32[]{:S(2)}, u32[]{:S(2)}) collective-permute-start(bf16[512,512]{1,0:T(8,128)(2,1)} %get-tuple-element.13), channel_id=1, source_target_pairs={{0,1},{1,0},{2,3},{3,2},{4,5},{5,4},{6,7},{7,6},{8,9},{9,8},{10,11... | collective-permute-start | bytes 1572872 | tf_op jit(solution)/shard_map/ppermute | solution.py:271
  180.3 0.8 copy-start.4
  189.1 47.1 %collective-permute-start.3 = (bf16[512,2048]{1,0:T(8,128)(2,1)}, bf16[512,2048]{1,0:T(8,128)(2,1)S(1)}, u32[]{:S(2)}, u32[]{:S(2)}) collective-permute-start(bf16[512,2048]{1,0:T(8,128)(2,1)} %get-tuple-element.15.x_ref), channel_id=1, source_target_pairs={{0,1},{1,0},{2,3},{3,2},{4,5},{5,4},{6,7},{7,6},{8,9},{9,8},{10,11... | collective-permute-start | bytes 6291464 | tf_op jit(solution)/shard_map/ppermute | solution.py:275
  249.5 31.0 %collective-permute-start.4 = (bf16[256,2048]{1,0:T(8,128)(2,1)}, bf16[256,2048]{1,0:T(8,128)(2,1)S(1)}, u32[]{:S(2)}, u32[]{:S(2)}) collective-permute-start(bf16[256,2048]{1,0:T(8,128)(2,1)} %ffn.4), channel_id=1, source_target_pairs={{0,1},{1,0},{2,3},{3,2},{4,5},{5,4},{6,7},{7,6},{8,9},{9,8},{10,11... | collective-permute-start | bytes 3145736 | tf_op jit(solution)/shard_map/ppermute | solution.py:281
  262.8 33.0 %collective-permute-start.5 = (bf16[256,2048]{1,0:T(8,128)(2,1)}, bf16[256,2048]{1,0:T(8,128)(2,1)S(1)}, u32[]{:S(2)}, u32[]{:S(2)}) collective-permute-start(bf16[256,2048]{1,0:T(8,128)(2,1)} %ffn.5), channel_id=1, source_target_pairs={{0,1},{1,0},{2,3},{3,2},{4,5},{5,4},{6,7},{7,6},{8,9},{9,8},{10,11... | collective-permute-start | bytes 3145736 | tf_op jit(solution)/shard_map/ppermute | solution.py:281
  263.4 34.8 %copy-start.6 = (f32[2048]{0:T(1024)S(1)}, f32[2048]{0:T(1024)}, u32[]{:S(2)}) copy-start(f32[2048]{0:T(1024)} %param.19) | copy-start | bytes 24580
  280.5 17.7 %copy-start.1 = (bf16[512,2048]{1,0:T(8,128)(2,1)S(1)}, bf16[512,2048]{1,0:T(8,128)(2,1)}, u32[]{:S(2)}) copy-start(bf16[512,2048]{1,0:T(8,128)(2,1)} %ffn.3) | copy-start | bytes 6291460
  280.5 17.7 %copy-start.3 = (bf16[512,2048]{1,0:T(8,128)(2,1)S(1)}, bf16[512,2048]{1,0:T(8,128)(2,1)}, u32[]{:S(2)}) copy-start(bf16[512,2048]{1,0:T(8,128)(2,1)} %get-tuple-element.14) | copy-start | bytes 6291460
Sparse Core Ops, SparseCore 0:
  9.6 64.1 all-gather.2
  75.4 97.5 all-gather.4

commit v2 on v1

--- a/solution.py
+++ b/solution.py
@@ -24,6 +24,10 @@
     while size % tile:
         tile -= LANES
     return tile
+
+
+def cost(flops):
+    return pl.CostEstimate(flops=flops, bytes_accessed=flops // 256, transcendentals=0)
 
 
 def one_minus_exp(y):
@@ -151,18 +155,24 @@
             wide, wide, wide, wide, wide, wide,
         ],
         compiler_params=pltpu.CompilerParams(vmem_limit_bytes=56 * 2**20),
+        cost_estimate=cost(32 * length * width * channels),
         name="mixer",
     )(place, own, other, gathered, gathered, conv_weight, w_rec, w_inp, slope)
 
 
-def out_kernel(ha_ref, hb_ref, wa_ref, wb_ref, tok_ref, gain_ref, mid_gain_ref, res_ref, mid_ref):
-    summed = dot_nt(ha_ref[...], wa_ref[...]) + dot_nt(hb_ref[...], wb_ref[...])
+def out_kernel(
+    ha_ref, hb_ref, wa_ref, wlow_ref, whigh_ref, tok_ref, gain_ref, mid_gain_ref, res_ref, mid_ref
+):
+    second = hb_ref[...]
+    summed = dot_nt(ha_ref[...], wa_ref[...]) + jnp.concatenate(
+        [dot_nt(second, wlow_ref[...]), dot_nt(second, whigh_ref[...])], axis=1
+    )
     residual = (tok_ref[...].astype(F32) + normed(summed, gain_ref[...])).astype(BF16)
     res_ref[...] = residual
     mid_ref[...] = normed(residual.astype(F32), mid_gain_ref[...]).astype(BF16)
 
 
-def out_projection(ha, hb, wa, wa_block, wb, wb_block, tokens, gain, mid_gain):
+def out_projection(ha, hb, wa, wa_block, wlow, wb_block, whigh, tokens, gain, mid_gain):
     rows, width = tokens.shape
     tile = min(rows, 256)
     channels = ha.shape[1]
@@ -176,7 +186,8 @@
             hidden,
             hidden,
             pl.BlockSpec((width, channels), lambda i: (0, wa_block)),
-            pl.BlockSpec((width, channels), lambda i: (0, wb_block)),
+            pl.BlockSpec((width // 2, channels), lambda i: (0, wb_block)),
+            pl.BlockSpec((width // 2, channels), lambda i: (0, wb_block)),
             wide,
             gains,
             gains,
@@ -184,8 +195,9 @@
         out_specs=[wide, wide],
         out_shape=[jax.ShapeDtypeStruct((rows, width), BF16)] * 2,
         compiler_params=pltpu.CompilerParams(vmem_limit_bytes=56 * 2**20),
+        cost_estimate=cost(16 * rows * width * channels),
         name="out_projection",
-    )(ha, hb, wa, wb, tokens, gain[None], mid_gain[None])
+    )(ha, hb, wa, wlow, whigh, tokens, gain[None], mid_gain[None])
 
 
 def ffn_kernel(x_ref, gate_ref, up_ref, down_ref, out_ref, acc_ref):
@@ -228,12 +240,48 @@
         out_shape=jax.ShapeDtypeStruct((count, width), BF16),
         scratch_shapes=[pltpu.VMEM((count, width), F32)],
         compiler_params=pltpu.CompilerParams(vmem_limit_bytes=56 * 2**20),
+        cost_estimate=cost(6 * count * width * hidden_units),
         name="ffn",
     )(rows, gathered, gathered, gathered)
 
 
+def finish_kernel(res_ref, own_ref, back_ref, gain_ref, *refs):
+    summed = own_ref[...].astype(F32) + back_ref[...].astype(F32)
+    layer = res_ref[...].astype(F32) + normed(summed, gain_ref[...])
+    refs[-1][...] = layer.astype(BF16)
+
+
+def finish(residual, own, back, gain, piece, earlier):
+    size, width = back.shape
+    tile = min(size, LANES)
+    tiles = size // tile
+    placed = pl.BlockSpec((tile, width), lambda i: (piece * tiles + i, 0))
+    operands = [residual, own, back, gain[None]]
+    specs = [
+        placed,
+        placed,
+        pl.BlockSpec((tile, width), lambda i: (i, 0)),
+        pl.BlockSpec((1, width), lambda i: (0, 0)),
+    ]
+    aliases = {}
+    if earlier is not None:
+        aliases = {len(operands): 0}
+        operands.append(earlier)
+        specs.append(pl.BlockSpec(memory_space=pl.ANY))
+    return pl.pallas_call(
+        finish_kernel,
+        grid=(tiles,),
+        in_specs=specs,
+        out_specs=placed,
+        out_shape=jax.ShapeDtypeStruct(residual.shape, BF16),
+        input_output_aliases=aliases,
+        name="finish",
+    )(*operands)
+
+
 def per_device(
     ranks,
+    fs_size,
     tokens,
     pre_mix_gain,
     post_mix_gain,
@@ -255,22 +303,43 @@
     mix_shard = jnp.concatenate([w_branch, w_gelu, out_weight_t], axis=1)
     ffn_shard = jnp.concatenate([w_gate, w_up, down_weight_t], axis=1)
     mix_all = lax.all_gather(mix_shard, "fs", axis=0, tiled=True)
-    mix_all, ffn_shard = lax.optimization_barrier((mix_all, ffn_shard))
-    ffn_all = lax.all_gather(ffn_shard, "fs", axis=0, tiled=True)
     channels = w_branch.shape[1]
     stream = tokens.astype(F32)
     normed_in = normed(stream, pre_mix_gain).astype(BF16)
+    if ranks == 2:
+        other_in = lax.ppermute(normed_in, "tp", swap)
+        mix_all, ffn_shard, other_in = lax.optimization_barrier((mix_all, ffn_shard, other_in))
+    else:
+        mix_all, ffn_shard = lax.optimization_barrier((mix_all, ffn_shard))
+    ffn_all = lax.all_gather(ffn_shard, "fs", axis=0, tiled=True)
     slope = -8.0 * jax.nn.softplus(-decay)
     place = lax.axis_index("tp").astype(jnp.int32).reshape(1)
     if ranks == 2:
-        other_in = lax.ppermute(normed_in, "tp", swap)
-        out_other = lax.ppermute(mix_all[:, 2 * channels :], "tp", swap)
+        lanes_at = 2 * channels
+        width = mix_all.shape[0]
+        pairs = fs_size % 2 == 0
+        if pairs:
+            part = lax.axis_index("fs").astype(jnp.int32) % 2
+            out_half = lax.dynamic_slice(
+                mix_all, (part * (width // 2), lanes_at), (width // 2, channels)
+            )
+        else:
+            out_half = mix_all[:, lanes_at:]
+        out_half = lax.ppermute(out_half, "tp", swap)
         mine, theirs = mixer(
             place, normed_in, other_in, mix_all, conv_weight, w_rec, w_inp, slope
         )
         received = lax.ppermute(theirs, "tp", swap)
+        if pairs:
+            mine, out_half = lax.optimization_barrier((mine, out_half))
+            neighbours = [(i, i ^ 1) for i in range(fs_size)]
+            out_next = lax.ppermute(out_half, "fs", neighbours)
+            out_low = jnp.where(part == 0, out_half, out_next)
+            out_high = jnp.where(part == 0, out_next, out_half)
+        else:
+            out_low, out_high = jnp.split(out_half, 2, axis=0)
         residual, normed_mid = out_projection(
-            mine, received, mix_all, 2, out_other, 0, tokens, post_mix_gain, pre_ffn_gain
+            mine, received, mix_all, 2, out_low, 0, out_high, tokens, post_mix_gain, pre_ffn_gain
         )
         other_mid = lax.ppermute(normed_mid, "tp", swap)
         pieces = 2 if rows % 512 == 0 else 1
@@ -280,7 +349,10 @@
             part = ffn(lax.slice_in_dim(other_mid, piece * size, (piece + 1) * size), ffn_all)
             returned.append(lax.ppermute(part, "tp", swap))
         own_part = ffn(normed_mid, ffn_all)
-        ffn_sum = own_part.astype(F32) + jnp.concatenate(returned, axis=0).astype(F32)
+        output = None
+        for piece in range(pieces):
+            output = finish(residual, own_part, returned[piece], post_ffn_gain, piece, output)
+        return output
     else:
         everything = lax.all_gather(normed_in, "tp", axis=0, tiled=True)
         half = everything.shape[0] // 2
@@ -293,7 +365,8 @@
         out_whole = lax.all_gather(mix_all[:, 2 * channels :], "tp", axis=1, tiled=True)
         mid_cols = hidden.shape[1] // 2
         residual, normed_mid = out_projection(
-            hidden[:, :mid_cols], hidden[:, mid_cols:], out_whole, 0, out_whole, 1,
+            hidden[:, :mid_cols], hidden[:, mid_cols:], out_whole, 0,
+            out_whole[: out_whole.shape[0] // 2], 1, out_whole[out_whole.shape[0] // 2 :],
             tokens, post_mix_gain, pre_ffn_gain,
         )
         every_mid = lax.all_gather(normed_mid, "tp", axis=0, tiled=True)
@@ -305,7 +378,7 @@
 
 def solution(mesh):
     return jax.shard_map(
-        functools.partial(per_device, mesh.shape["tp"]),
+        functools.partial(per_device, mesh.shape["tp"], mesh.shape["fs"]),
         mesh=mesh,
         in_specs=(
             P(("fs", "tp"), None),

time: 308 us -> 249 us (0.81)
  waiting for transfers between devices: 190 us -> 128 us
  Pallas kernels: 78.4 us -> 84.6 us
  other arithmetic: 12.6 us -> 9.16 us
    all_gather x1, waiting for transfers between devices: 62.8 us -> 12.4 us  [per_device(): mix_all = lax.all_gather(mix_shard, 'fs', axis=0, tiled=True)]
    ppermute x1, waiting for transfers between devices: 22.9 us -> 9.93 us  [per_device(): received = lax.ppermute(theirs, 'tp', swap)]
    pallas_call x0 -> x2, Pallas kernels: none -> 6.39 us  [finish(): pl.pallas_call(finish_kernel, grid=(tiles,), in_specs=specs, out_specs=pl...]
    ppermute x2, waiting for transfers between devices: 15.3 us -> 11.4 us  [per_device(): returned.append(lax.ppermute(part, 'tp', swap))]
  transfers between devices with their start and end apart: 8 -> 9, of which waited for: 5 -> 6; matrix products, arithmetic and copies ran while one was open for 3% -> 4% of each run, Pallas kernels for 22% -> 28%
where the time goes in v2:
time: 249 us
  waiting for transfers between devices  128 us (51%)
  Pallas kernels  84.6 us (34%)
  between operations  13.5 us (5%)
  other arithmetic  9.16 us (4%)
  starting transfers between devices  7.9 us (3%)
  local copies, waits for them, and re-layouts  5.59 us (2%)
    ppermute x1, waiting for transfers between devices, per_device(): other_mid = lax.ppermute(normed_mid, 'tp', swap)  46.8 us
    ppermute x1, waiting for transfers between devices, per_device(): other_in = lax.ppermute(normed_in, 'tp', swap)  44.7 us
    pallas_call x3, Pallas kernels, ffn(): pl.pallas_call(ffn_kernel, grid=(tiles,), in_specs=[whole, pl.BlockSpec((...  40.7 us
    pallas_call x1, Pallas kernels, mixer(): pl.pallas_call(mixer_kernel, grid=(count,), in_specs=[pl.BlockSpec(memory...  29.6 us
    all_gather x1, waiting for transfers between devices, per_device(): mix_all = lax.all_gather(mix_shard, 'fs', axis=0, tiled=True)  12.4 us
    ppermute x2, waiting for transfers between devices, per_device(): returned.append(lax.ppermute(part, 'tp', swap))  11.4 us
    ppermute x1, waiting for transfers between devices, per_device(): received = lax.ppermute(theirs, 'tp', swap)  9.93 us
    pallas_call x1, Pallas kernels, out_projection(): pl.pallas_call(out_kernel, grid=(rows // tile,), in_specs=[hidden, hidden...  7.93 us
  transfers between devices with their start and end apart: 9, of which 6 were waited for; matrix products, arithmetic and copies ran while one was open for 4% of the time, Pallas kernels for 28%

profile of v2, /device:TPU:0, one launch (start us, length us, event | category | flops | bytes accessed | tf_op | source)
XLA Modules:
  0.0 248.6 jit_solution(3992266499417542521)
XLA Ops:
  6.5 0.0 copy-start.6
  6.5 0.0 all-gather.3.cloned.1.call-start
  6.5 2.0 pad_maximum_fusion.1
  8.5 0.0 all-gather.3.cloned.1.call-update
  8.5 0.0 all-gather.5.cloned.1.call-start
  8.6 2.1 fusion
  10.7 0.0 copy-done
  10.7 0.0 copy-done.6
  10.7 0.0 copy-start.3
  10.7 0.0 copy-start.4
  10.7 0.0 copy-start.5
  10.7 1.9 fusion.2.own_ref
  12.6 3.0 %collective-permute-start = (bf16[512,2048]{1,0:T(8,128)(2,1)}, bf16[512,2048]{1,0:T(8,128)(2,1)S(1)}, u32[]{:S(2)}, u32[]{:S(2)}) collective-permute-start(bf16[512,2048]{1,0:T(8,128)(2,1)} %fusion.2.own_ref), channel_id=1, source_target_pairs={{0,1},{1,0},{2,3},{3,2},{4,5},{5,4},{6,7},{7,6},{8,9},{9,8},{10,11... | collective-permute-start | bytes 6291464 | tf_op jit(solution)/shard_map/ppermute | solution.py:310
  15.5 0.0 copy-done.3
  15.5 0.0 copy-done.4
  15.5 0.0 copy-done.5
  15.6 1.1 pad_maximum_fusion
  16.7 44.7 %collective-permute-done.other_ref = bf16[512,2048]{1,0:T(8,128)(2,1)S(1)} collective-permute-done((bf16[512,2048]{1,0:T(8,128)(2,1)}, bf16[512,2048]{1,0:T(8,128)(2,1)S(1)}, u32[]{:S(2)}, u32[]{:S(2)}) %collective-permute-start) | collective-permute-done | bytes 2097184 | tf_op jit(solution)/shard_map/ppermute | solution.py:310
  61.4 12.4 %all-gather.3.cloned.1.call-done.wb_ref.wg_ref.wa_ref = bf16[2048,1536]{1,0:T(8,128)(2,1)} async-done(((bf16[128,1536]{1,0:T(8,128)(2,1)}), bf16[2048,1536]{1,0:T(8,128)(2,1)}) %all-gather.3.cloned.1.call-update) | async-done | bytes 6291472 | tf_op jit(solution)/shard_map/all_gather | solution.py:305
  73.8 0.0 all-gather.5.cloned.1.call-update
  73.8 0.0 copy-done.7
  73.8 0.6 fusion.3.slope_ref
  74.4 1.3 constant_dynamic-slice_fusion
  75.7 1.5 collective-permute-start.1
  77.3 0.0 copy-done.8
  77.3 29.6 %mixer.1 = (bf16[512,512]{1,0:T(8,128)(2,1)}, bf16[512,512]{1,0:T(8,128)(2,1)}) custom-call(s32[1]{0:T(128)} %bitcast.place_ref, bf16[512,2048]{1,0:T(8,128)(2,1)} %fusion.2.own_ref, bf16[512,2048]{1,0:T(8,128)(2,1)} %copy-done.8, bf16[2048,1536]{1,0:T(8,128)(2,1)} %all-gather.3.cloned.1.call-done.wb_ref.wg_ref.wa_ref, ...), custom_call_target="tpu_custom_call" | custom-call | flops 34359738368 | bytes 134217728 | tf_op jit(solution)/shard_map/mixer/pallas_call | solution.py:136
  106.9 0.0 collective-permute-done.1
  106.9 0.1 collective-permute-start.3
  107.0 0.6 collective-permute-start.2
  107.6 2.4 collective-permute-done.3
  110.0 1.5 broadcast_select_fusion
  111.6 9.9 %collective-permute-done.2.hb_ref = bf16[512,512]{1,0:T(8,128)(2,1)S(1)} collective-permute-done((bf16[512,512]{1,0:T(8,128)(2,1)}, bf16[512,512]{1,0:T(8,128)(2,1)S(1)}, u32[]{:S(2)}, u32[]{:S(2)}) %collective-permute-start.2) | collective-permute-done | bytes 524320 | tf_op jit(solution)/shard_map/ppermute | solution.py:332
  121.5 0.8 copy-done.9
  122.3 7.9 %out_projection.1 = (bf16[512,2048]{1,0:T(8,128)(2,1)}, bf16[512,2048]{1,0:T(8,128)(2,1)}) custom-call(bf16[512,512]{1,0:T(8,128)(2,1)} %get-tuple-element.17.ha_ref, bf16[512,512]{1,0:T(8,128)(2,1)} %copy-done.9, bf16[2048,1536]{1,0:T(8,128)(2,1)} %all-gather.3.cloned.1.call-done.wb_ref.wg_ref.wa_ref, bf16[1024,512]{1,0:T(8,128)(2,1)} %get-tuple-element.26.wlow_ref, ...), custom_call_target="tpu_custom_call" | custom-call | flops 8589934592 | bytes 33554432 | tf_op jit(solution)/shard_map/out_projection/pallas_call | solution.py:182
  130.3 0.6 collective-permute-start.4
  130.9 46.8 %collective-permute-done.4 = bf16[512,2048]{1,0:T(8,128)(2,1)S(1)} collective-permute-done((bf16[512,2048]{1,0:T(8,128)(2,1)}, bf16[512,2048]{1,0:T(8,128)(2,1)S(1)}, u32[]{:S(2)}, u32[]{:S(2)}) %collective-permute-start.4) | collective-permute-done | bytes 2097184 | tf_op jit(solution)/shard_map/ppermute | solution.py:344
  177.7 1.5 fusion.4
  179.2 11.8 %ffn.5 = bf16[256,2048]{1,0:T(8,128)(2,1)} custom-call(bf16[256,2048]{1,0:T(8,128)(2,1)} %get-tuple-element.23.x_ref, bf16[2048,4608]{1,0:T(8,128)(2,1)} %all-gather.5.cloned.1.call-done.gate_ref.up_ref.down_ref, bf16[2048,4608]{1,0:T(8,128)(2,1)} %all-gather.5.cloned.1.call-done.gate_ref.up_ref.down_ref, ...), custom_call_target="tpu_custom_call" | custom-call | flops 4831838208 | bytes 18874368 | tf_op jit(solution)/shard_map/ffn/pallas_call | solution.py:230
  191.0 0.5 collective-permute-start.6
  191.6 11.8 %ffn.4 = bf16[256,2048]{1,0:T(8,128)(2,1)} custom-call(bf16[256,2048]{1,0:T(8,128)(2,1)} %get-tuple-element.24.x_ref, bf16[2048,4608]{1,0:T(8,128)(2,1)} %all-gather.5.cloned.1.call-done.gate_ref.up_ref.down_ref, bf16[2048,4608]{1,0:T(8,128)(2,1)} %all-gather.5.cloned.1.call-done.gate_ref.up_ref.down_ref, ...), custom_call_target="tpu_custom_call" | custom-call | flops 4831838208 | bytes 18874368 | tf_op jit(solution)/shard_map/ffn/pallas_call | solution.py:230
  203.4 1.5 collective-permute-start.5
  204.9 17.1 %ffn.3.own_ref = bf16[512,2048]{1,0:T(8,128)(2,1)} custom-call(bf16[512,2048]{1,0:T(8,128)(2,1)} %get-tuple-element.21.x_ref, bf16[2048,4608]{1,0:T(8,128)(2,1)} %all-gather.5.cloned.1.call-done.gate_ref.up_ref.down_ref, bf16[2048,4608]{1,0:T(8,128)(2,1)} %all-gather.5.cloned.1.call-done.gate_ref.up_ref.down_ref, ...), custom_call_target="tpu_custom_call" | custom-call | flops 9663676416 | bytes 37748736 | tf_op jit(solution)/shard_map/ffn/pallas_call | solution.py:230
  221.9 0.0 collective-permute-done.6.back_ref
  221.9 1.0 copy-done.1
  222.9 3.3 %finish.2.refs_0_ = bf16[512,2048]{1,0:T(8,128)(2,1)} custom-call(bf16[512,2048]{1,0:T(8,128)(2,1)} %get-tuple-element.20.res_ref, bf16[512,2048]{1,0:T(8,128)(2,1)} %ffn.3.own_ref, bf16[256,2048]{1,0:T(8,128)(2,1)} %copy-done.1, f32[1,2048]{1,0:T(1,128)} %bitcast.4), custom_call_target="tpu_custom_call" | custom-call | tf_op jit(solution)/shard_map/finish/pallas_call | solution.py:271
  226.2 11.4 %collective-permute-done.5.back_ref = bf16[256,2048]{1,0:T(8,128)(2,1)S(1)} collective-permute-done((bf16[256,2048]{1,0:T(8,128)(2,1)}, bf16[256,2048]{1,0:T(8,128)(2,1)S(1)}, u32[]{:S(2)}, u32[]{:S(2)}) %collective-permute-start.5) | collective-permute-done | bytes 1048608 | tf_op jit(solution)/shard_map/ppermute | solution.py:350
  237.6 1.0 copy-done.2
  238.6 3.1 %finish.3 = bf16[512,2048]{1,0:T(8,128)(2,1)} custom-call(bf16[512,2048]{1,0:T(8,128)(2,1)} %get-tuple-element.20.res_ref, bf16[512,2048]{1,0:T(8,128)(2,1)} %ffn.3.own_ref, bf16[256,2048]{1,0:T(8,128)(2,1)} %copy-done.2, f32[1,2048]{1,0:T(1,128)} %bitcast.5, bf16[512,2048]{1,0:T(8,128)(2,1)} %finish.2.refs_0_), custom_call_target="tpu_custom_call", output_to_operand_aliasing={{}: (4, {})} | custom-call | tf_op jit(solution)/shard_map/finish/pallas_call | solution.py:271
  (8 shorter events, 0.0 us)
Async XLA Ops:
  6.5 4.1 %copy-start = (bf16[512,2048]{1,0:T(8,128)(2,1)S(1)}, bf16[512,2048]{1,0:T(8,128)(2,1)}, u32[]{:S(2)}) copy-start(bf16[512,2048]{1,0:T(8,128)(2,1)} %tok_ref.1) | copy-start | bytes 6291460
  6.5 4.1 %copy-start.6 = (f32[2048]{0:T(1024)S(1)}, f32[2048]{0:T(1024)}, u32[]{:S(2)}) copy-start(f32[2048]{0:T(1024)} %param.16) | copy-start | bytes 24580
  6.5 67.2 %all-gather.3.cloned.1.call-start = ((), (), s32[]{:S(2)}) async-start(), calls=%async_computation | async-start | bytes 6684672 | tf_op jit(solution)/shard_map/all_gather | solution.py:305
  8.5 170.7 %all-gather.5.cloned.1.call-start = ((), (), s32[]{:S(2)}) async-start(), calls=%async_computation.1 | async-start | bytes 20054016 | tf_op jit(solution)/shard_map/all_gather | solution.py:314
  10.7 4.9 %copy-start.3 = (bf16[128,1536]{1,0:T(8,128)(2,1)S(1)}, bf16[128,1536]{1,0:T(8,128)(2,1)}, u32[]{:S(2)}) copy-start(bf16[128,1536]{1,0:T(8,128)(2,1)} %param.29) | copy-start | bytes 1179652
  10.7 4.9 %copy-start.4 = (bf16[128,1536]{1,0:T(8,128)(2,1)S(1)}, bf16[128,1536]{1,0:T(8,128)(2,1)}, u32[]{:S(2)}) copy-start(bf16[128,1536]{1,0:T(8,128)(2,1)} %param.28) | copy-start | bytes 1179652
  10.7 4.9 %copy-start.5 = (bf16[128,1536]{1,0:T(8,128)(2,1)S(1)}, bf16[128,1536]{1,0:T(8,128)(2,1)}, u32[]{:S(2)}) copy-start(bf16[128,1536]{1,0:T(8,128)(2,1)} %param.27) | copy-start | bytes 1179652
  12.6 61.2 %copy-start.7 = (f32[2,512]{1,0:T(2,128)S(1)}, f32[2,512]{1,0:T(2,128)}, u32[]{:S(2)}) copy-start(f32[2,512]{1,0:T(2,128)} %param.25) | copy-start | bytes 12292
  12.6 48.8 %collective-permute-start = (bf16[512,2048]{1,0:T(8,128)(2,1)}, bf16[512,2048]{1,0:T(8,128)(2,1)S(1)}, u32[]{:S(2)}, u32[]{:S(2)}) collective-permute-start(bf16[512,2048]{1,0:T(8,128)(2,1)} %fusion.2.own_ref), channel_id=1, source_target_pairs={{0,1},{1,0},{2,3},{3,2},{4,5},{5,4},{6,7},{7,6},{8,9},{9,8},{10,11... | collective-permute-start | bytes 6291464 | tf_op jit(solution)/shard_map/ppermute | solution.py:310
  61.4 15.9 %copy-start.8 = (bf16[512,2048]{1,0:T(8,128)(2,1)}, bf16[512,2048]{1,0:T(8,128)(2,1)S(1)}, u32[]{:S(2)}) copy-start(bf16[512,2048]{1,0:T(8,128)(2,1)S(1)} %collective-permute-done.other_ref) | copy-start | bytes 6291460
  75.7 31.2 %collective-permute-start.1 = (bf16[1024,512]{1,0:T(8,128)(2,1)S(1)}, bf16[1024,512]{1,0:T(8,128)(2,1)S(1)}, u32[]{:S(2)}, u32[]{:S(2)}) collective-permute-start(bf16[1024,512]{1,0:T(8,128)(2,1)S(1)} %constant_dynamic-slice_fusion), channel_id=1, source_target_pairs={{0,1},{1,0},{2,3},{3,2},{4,5},{5,4},{6,7},{7,6},{8,9},{9,8},{10,11... | collective-permute-start | bytes 3145736 | tf_op jit(solution)/shard_map/ppermute | solution.py:328
  106.9 3.1 %collective-permute-start.3 = (bf16[1024,512]{1,0:T(8,128)(2,1)S(1)}, bf16[1024,512]{1,0:T(8,128)(2,1)S(1)}, u32[]{:S(2)}, u32[]{:S(2)}) collective-permute-start(bf16[1024,512]{1,0:T(8,128)(2,1)S(1)} %collective-permute-done.1), channel_id=1, source_target_pairs={{0,2},{2,0},{4,6},{6,4},{8,10},{10,8},{12,14},{14,12},{16,18},{18,... | collective-permute-start | bytes 3145736 | tf_op jit(solution)/shard_map/ppermute | solution.py:336
  107.0 14.5 %collective-permute-start.2 = (bf16[512,512]{1,0:T(8,128)(2,1)}, bf16[512,512]{1,0:T(8,128)(2,1)S(1)}, u32[]{:S(2)}, u32[]{:S(2)}) collective-permute-start(bf16[512,512]{1,0:T(8,128)(2,1)} %get-tuple-element.18), channel_id=1, source_target_pairs={{0,1},{1,0},{2,3},{3,2},{4,5},{5,4},{6,7},{7,6},{8,9},{9,8},{10,11... | collective-permute-start | bytes 1572872 | tf_op jit(solution)/shard_map/ppermute | solution.py:332
  121.5 0.8 copy-start.9
  130.3 47.5 %collective-permute-start.4 = (bf16[512,2048]{1,0:T(8,128)(2,1)}, bf16[512,2048]{1,0:T(8,128)(2,1)S(1)}, u32[]{:S(2)}, u32[]{:S(2)}) collective-permute-start(bf16[512,2048]{1,0:T(8,128)(2,1)} %get-tuple-element.21.x_ref), channel_id=1, source_target_pairs={{0,1},{1,0},{2,3},{3,2},{4,5},{5,4},{6,7},{7,6},{8,9},{9,8},{10,11... | collective-permute-start | bytes 6291464 | tf_op jit(solution)/shard_map/ppermute | solution.py:344
  191.0 30.9 %collective-permute-start.6 = (bf16[256,2048]{1,0:T(8,128)(2,1)}, bf16[256,2048]{1,0:T(8,128)(2,1)S(1)}, u32[]{:S(2)}, u32[]{:S(2)}) collective-permute-start(bf16[256,2048]{1,0:T(8,128)(2,1)} %ffn.5), channel_id=1, source_target_pairs={{0,1},{1,0},{2,3},{3,2},{4,5},{5,4},{6,7},{7,6},{8,9},{9,8},{10,11... | collective-permute-start | bytes 3145736 | tf_op jit(solution)/shard_map/ppermute | solution.py:350
  203.4 34.2 %collective-permute-start.5 = (bf16[256,2048]{1,0:T(8,128)(2,1)}, bf16[256,2048]{1,0:T(8,128)(2,1)S(1)}, u32[]{:S(2)}, u32[]{:S(2)}) collective-permute-start(bf16[256,2048]{1,0:T(8,128)(2,1)} %ffn.4), channel_id=1, source_target_pairs={{0,1},{1,0},{2,3},{3,2},{4,5},{5,4},{6,7},{7,6},{8,9},{9,8},{10,11... | collective-permute-start | bytes 3145736 | tf_op jit(solution)/shard_map/ppermute | solution.py:350
  221.9 1.0 copy-start.1
  237.6 1.0 copy-start.2
Sparse Core Ops, SparseCore 0:
  9.6 64.1 all-gather.2
  75.4 97.5 all-gather.4

commit v3 on v2

--- a/solution.py
+++ b/solution.py
@@ -341,12 +341,15 @@
         residual, normed_mid = out_projection(
             mine, received, mix_all, 2, out_low, 0, out_high, tokens, post_mix_gain, pre_ffn_gain
         )
-        other_mid = lax.ppermute(normed_mid, "tp", swap)
         pieces = 2 if rows % 512 == 0 else 1
         size = rows // pieces
         returned = []
+        crossed = [
+            lax.ppermute(lax.slice_in_dim(normed_mid, i * size, (i + 1) * size), "tp", swap)
+            for i in range(pieces)
+        ]
         for piece in range(pieces):
-            part = ffn(lax.slice_in_dim(other_mid, piece * size, (piece + 1) * size), ffn_all)
+            part = ffn(crossed[piece], ffn_all)
             returned.append(lax.ppermute(part, "tp", swap))
         own_part = ffn(normed_mid, ffn_all)
         output = None

time: 249 us -> 244 us (0.980)
  waiting for transfers between devices: 128 us -> 120 us
    ppermute x1 -> x2, waiting for transfers between devices: 46.8 us -> 24 us  [per_device(): lax.ppermute(lax.slice_in_dim(normed_mid, i * size, (i + 1) * size), 'tp'...]
    all_gather x1, waiting for transfers between devices: 0.01 us -> 14.9 us  [per_device(): ffn_all = lax.all_gather(ffn_shard, 'fs', axis=0, tiled=True)]
  transfers between devices with their start and end apart: 9 -> 10, of which waited for: 6 -> 7; matrix products, arithmetic and copies ran while one was open for 4% -> 4% of each run, Pallas kernels for 28% -> 33%
where the time goes in v3:
time: 244 us
  waiting for transfers between devices  120 us (49%)
  Pallas kernels  84.7 us (35%)
  between operations  13.5 us (6%)
  starting transfers between devices  9.35 us (4%)
  other arithmetic  9.15 us (4%)
  local copies, waits for them, and re-layouts  6.9 us (3%)
    ppermute x1, waiting for transfers between devices, per_device(): other_in = lax.ppermute(normed_in, 'tp', swap)  44.7 us
    pallas_call x3, Pallas kernels, ffn(): pl.pallas_call(ffn_kernel, grid=(tiles,), in_specs=[whole, pl.BlockSpec((...  40.8 us
    pallas_call x1, Pallas kernels, mixer(): pl.pallas_call(mixer_kernel, grid=(count,), in_specs=[pl.BlockSpec(memory...  29.6 us
    ppermute x2, waiting for transfers between devices, per_device(): lax.ppermute(lax.slice_in_dim(normed_mid, i * size, (i + 1) * size), 'tp'...  24 us
    all_gather x1, waiting for transfers between devices, per_device(): ffn_all = lax.all_gather(ffn_shard, 'fs', axis=0, tiled=True)  14.9 us
    all_gather x1, waiting for transfers between devices, per_device(): mix_all = lax.all_gather(mix_shard, 'fs', axis=0, tiled=True)  12.4 us
    ppermute x2, waiting for transfers between devices, per_device(): returned.append(lax.ppermute(part, 'tp', swap))  11.8 us
    ppermute x1, waiting for transfers between devices, per_device(): received = lax.ppermute(theirs, 'tp', swap)  9.93 us
  transfers between devices with their start and end apart: 10, of which 7 were waited for; matrix products, arithmetic and copies ran while one was open for 4% of the time, Pallas kernels for 33%

profile of v3, /device:TPU:0, one launch (start us, length us, event | category | flops | bytes accessed | tf_op | source)
XLA Modules:
  0.0 243.9 jit_solution(5511385200832110786)
XLA Ops:
  6.5 0.0 all-gather.3.cloned.1.call-start
  6.5 1.9 pad_maximum_fusion.1
  8.5 0.0 all-gather.3.cloned.1.call-update
  8.5 0.0 all-gather.5.cloned.1.call-start
  8.6 2.1 fusion
  10.7 0.0 copy-done
  10.7 0.0 copy-done.8
  10.7 0.0 copy-start.5
  10.7 0.0 copy-start.6
  10.7 0.0 copy-start.7
  10.7 1.9 fusion.2.own_ref
  12.6 3.0 %collective-permute-start = (bf16[512,2048]{1,0:T(8,128)(2,1)}, bf16[512,2048]{1,0:T(8,128)(2,1)S(1)}, u32[]{:S(2)}, u32[]{:S(2)}) collective-permute-start(bf16[512,2048]{1,0:T(8,128)(2,1)} %fusion.2.own_ref), channel_id=1, source_target_pairs={{0,1},{1,0},{2,3},{3,2},{4,5},{5,4},{6,7},{7,6},{8,9},{9,8},{10,11... | collective-permute-start | bytes 6291464 | tf_op jit(solution)/shard_map/ppermute | solution.py:310
  15.5 0.0 copy-done.5
  15.5 0.0 copy-done.6
  15.5 1.1 pad_maximum_fusion
  16.6 44.7 %collective-permute-done.other_ref = bf16[512,2048]{1,0:T(8,128)(2,1)S(1)} collective-permute-done((bf16[512,2048]{1,0:T(8,128)(2,1)}, bf16[512,2048]{1,0:T(8,128)(2,1)S(1)}, u32[]{:S(2)}, u32[]{:S(2)}) %collective-permute-start) | collective-permute-done | bytes 2097184 | tf_op jit(solution)/shard_map/ppermute | solution.py:310
  61.4 12.4 %all-gather.3.cloned.1.call-done.wb_ref.wg_ref.wa_ref = bf16[2048,1536]{1,0:T(8,128)(2,1)} async-done(((bf16[128,1536]{1,0:T(8,128)(2,1)}), bf16[2048,1536]{1,0:T(8,128)(2,1)}) %all-gather.3.cloned.1.call-update) | async-done | bytes 6291472 | tf_op jit(solution)/shard_map/all_gather | solution.py:305
  73.8 0.0 all-gather.5.cloned.1.call-update
  73.8 0.6 fusion.3.slope_ref
  74.4 1.3 constant_dynamic-slice_fusion
  75.7 1.5 collective-permute-start.1
  77.3 29.6 %mixer.1 = (bf16[512,512]{1,0:T(8,128)(2,1)}, bf16[512,512]{1,0:T(8,128)(2,1)}) custom-call(s32[1]{0:T(128)} %bitcast.place_ref, bf16[512,2048]{1,0:T(8,128)(2,1)} %fusion.2.own_ref, bf16[512,2048]{1,0:T(8,128)(2,1)} %copy-done.10, bf16[2048,1536]{1,0:T(8,128)(2,1)} %all-gather.3.cloned.1.call-done.wb_ref.wg_ref.wa_ref, ...), custom_call_target="tpu_custom_call" | custom-call | flops 34359738368 | bytes 134217728 | tf_op jit(solution)/shard_map/mixer/pallas_call | solution.py:136
  106.9 0.0 collective-permute-done.1
  106.9 0.1 collective-permute-start.3
  107.0 0.6 collective-permute-start.2
  107.6 2.5 %collective-permute-done.3 = bf16[1024,512]{1,0:T(8,128)(2,1)S(1)} collective-permute-done((bf16[1024,512]{1,0:T(8,128)(2,1)S(1)}, bf16[1024,512]{1,0:T(8,128)(2,1)S(1)}, u32[]{:S(2)}, u32[]{:S(2)}) %collective-permute-start.3) | collective-permute-done | bytes 1048608 | tf_op jit(solution)/shard_map/ppermute | solution.py:336
  110.0 1.5 broadcast_select_fusion
  111.6 9.9 %collective-permute-done.2.hb_ref = bf16[512,512]{1,0:T(8,128)(2,1)S(1)} collective-permute-done((bf16[512,512]{1,0:T(8,128)(2,1)}, bf16[512,512]{1,0:T(8,128)(2,1)S(1)}, u32[]{:S(2)}, u32[]{:S(2)}) %collective-permute-start.2) | collective-permute-done | bytes 524320 | tf_op jit(solution)/shard_map/ppermute | solution.py:332
  121.5 0.8 copy-done.11
  122.3 7.9 %out_projection.1 = (bf16[512,2048]{1,0:T(8,128)(2,1)}, bf16[512,2048]{1,0:T(8,128)(2,1)}) custom-call(bf16[512,512]{1,0:T(8,128)(2,1)} %get-tuple-element.17.ha_ref, bf16[512,512]{1,0:T(8,128)(2,1)} %copy-done.11, bf16[2048,1536]{1,0:T(8,128)(2,1)} %all-gather.3.cloned.1.call-done.wb_ref.wg_ref.wa_ref, bf16[1024,512]{1,0:T(8,128)(2,1)} %get-tuple-element.26.wlow_ref, ...), custom_call_target="tpu_custom_call" | custom-call | flops 8589934592 | bytes 33554432 | tf_op jit(solution)/shard_map/out_projection/pallas_call | solution.py:182
  130.3 1.8 fusion.4
  132.0 0.6 collective-permute-start.6
  132.6 1.5 collective-permute-start.4
  134.1 24.0 %collective-permute-done.6.x_ref = bf16[256,2048]{1,0:T(8,128)(2,1)S(1)} collective-permute-done((bf16[256,2048]{1,0:T(8,128)(2,1)S(1)}, bf16[256,2048]{1,0:T(8,128)(2,1)S(1)}, u32[]{:S(2)}, u32[]{:S(2)}) %collective-permute-start.6) | collective-permute-done | bytes 1048608 | tf_op jit(solution)/shard_map/ppermute | solution.py:348
  158.1 14.9 %all-gather.5.cloned.1.call-done.gate_ref.up_ref.down_ref = bf16[2048,4608]{1,0:T(8,128)(2,1)} async-done(((bf16[128,4608]{1,0:T(8,128)(2,1)}), bf16[2048,4608]{1,0:T(8,128)(2,1)}) %all-gather.5.cloned.1.call-update) | async-done | bytes 18874384 | tf_op jit(solution)/shard_map/all_gather | solution.py:314
  173.0 11.9 %ffn.5 = bf16[256,2048]{1,0:T(8,128)(2,1)} custom-call(bf16[256,2048]{1,0:T(8,128)(2,1)} %copy-done.2, bf16[2048,4608]{1,0:T(8,128)(2,1)} %all-gather.5.cloned.1.call-done.gate_ref.up_ref.down_ref, bf16[2048,4608]{1,0:T(8,128)(2,1)} %all-gather.5.cloned.1.call-done.gate_ref.up_ref.down_ref, ...), custom_call_target="tpu_custom_call" | custom-call | flops 4831838208 | bytes 18874368 | tf_op jit(solution)/shard_map/ffn/pallas_call | solution.py:230
  184.9 1.5 collective-permute-start.7
  186.4 0.0 collective-permute-done.4.x_ref
  186.4 1.0 copy-done.1
  187.4 11.8 %ffn.4 = bf16[256,2048]{1,0:T(8,128)(2,1)} custom-call(bf16[256,2048]{1,0:T(8,128)(2,1)} %copy-done.1, bf16[2048,4608]{1,0:T(8,128)(2,1)} %all-gather.5.cloned.1.call-done.gate_ref.up_ref.down_ref, bf16[2048,4608]{1,0:T(8,128)(2,1)} %all-gather.5.cloned.1.call-done.gate_ref.up_ref.down_ref, ...), custom_call_target="tpu_custom_call" | custom-call | flops 4831838208 | bytes 18874368 | tf_op jit(solution)/shard_map/ffn/pallas_call | solution.py:230
  199.2 0.6 collective-permute-start.5
  199.8 17.1 %ffn.3.own_ref = bf16[512,2048]{1,0:T(8,128)(2,1)} custom-call(bf16[512,2048]{1,0:T(8,128)(2,1)} %get-tuple-element.21.x_ref, bf16[2048,4608]{1,0:T(8,128)(2,1)} %all-gather.5.cloned.1.call-done.gate_ref.up_ref.down_ref, bf16[2048,4608]{1,0:T(8,128)(2,1)} %all-gather.5.cloned.1.call-done.gate_ref.up_ref.down_ref, ...), custom_call_target="tpu_custom_call" | custom-call | flops 9663676416 | bytes 37748736 | tf_op jit(solution)/shard_map/ffn/pallas_call | solution.py:230
  216.8 0.0 collective-permute-done.7.back_ref
  216.8 1.0 copy-done.3
  217.8 3.2 %finish.2.refs_0_ = bf16[512,2048]{1,0:T(8,128)(2,1)} custom-call(bf16[512,2048]{1,0:T(8,128)(2,1)} %get-tuple-element.20.res_ref, bf16[512,2048]{1,0:T(8,128)(2,1)} %ffn.3.own_ref, bf16[256,2048]{1,0:T(8,128)(2,1)} %copy-done.3, f32[1,2048]{1,0:T(1,128)} %bitcast.4), custom_call_target="tpu_custom_call" | custom-call | tf_op jit(solution)/shard_map/finish/pallas_call | solution.py:271
  221.0 11.8 %collective-permute-done.5.back_ref = bf16[256,2048]{1,0:T(8,128)(2,1)S(1)} collective-permute-done((bf16[256,2048]{1,0:T(8,128)(2,1)}, bf16[256,2048]{1,0:T(8,128)(2,1)S(1)}, u32[]{:S(2)}, u32[]{:S(2)}) %collective-permute-start.5) | collective-permute-done | bytes 1048608 | tf_op jit(solution)/shard_map/ppermute | solution.py:353
  232.9 1.0 copy-done.4
  233.9 3.1 %finish.3 = bf16[512,2048]{1,0:T(8,128)(2,1)} custom-call(bf16[512,2048]{1,0:T(8,128)(2,1)} %get-tuple-element.20.res_ref, bf16[512,2048]{1,0:T(8,128)(2,1)} %ffn.3.own_ref, bf16[256,2048]{1,0:T(8,128)(2,1)} %copy-done.4, f32[1,2048]{1,0:T(1,128)} %bitcast.5, bf16[512,2048]{1,0:T(8,128)(2,1)} %finish.2.refs_0_), custom_call_target="tpu_custom_call", output_to_operand_aliasing={{}: (4, {})} | custom-call | tf_op jit(solution)/shard_map/finish/pallas_call | solution.py:271
  (14 shorter events, 0.0 us)
Async XLA Ops:
  6.5 4.1 %copy-start = (bf16[512,2048]{1,0:T(8,128)(2,1)S(1)}, bf16[512,2048]{1,0:T(8,128)(2,1)}, u32[]{:S(2)}) copy-start(bf16[512,2048]{1,0:T(8,128)(2,1)} %tok_ref.1) | copy-start | bytes 6291460
  6.5 4.1 %copy-start.8 = (f32[2048]{0:T(1024)S(1)}, f32[2048]{0:T(1024)}, u32[]{:S(2)}) copy-start(f32[2048]{0:T(1024)} %param.16) | copy-start | bytes 24580
  6.5 67.2 %all-gather.3.cloned.1.call-start = ((), (), s32[]{:S(2)}) async-start(), calls=%async_computation | async-start | bytes 6684672 | tf_op jit(solution)/shard_map/all_gather | solution.py:305
  8.5 164.5 %all-gather.5.cloned.1.call-start = ((), (), s32[]{:S(2)}) async-start(), calls=%async_computation.1 | async-start | bytes 20054016 | tf_op jit(solution)/shard_map/all_gather | solution.py:314
  10.7 4.9 %copy-start.5 = (bf16[128,1536]{1,0:T(8,128)(2,1)S(1)}, bf16[128,1536]{1,0:T(8,128)(2,1)}, u32[]{:S(2)}) copy-start(bf16[128,1536]{1,0:T(8,128)(2,1)} %param.29) | copy-start | bytes 1179652
  10.7 4.9 %copy-start.6 = (bf16[128,1536]{1,0:T(8,128)(2,1)S(1)}, bf16[128,1536]{1,0:T(8,128)(2,1)}, u32[]{:S(2)}) copy-start(bf16[128,1536]{1,0:T(8,128)(2,1)} %param.28) | copy-start | bytes 1179652
  10.7 4.9 %copy-start.7 = (bf16[128,1536]{1,0:T(8,128)(2,1)S(1)}, bf16[128,1536]{1,0:T(8,128)(2,1)}, u32[]{:S(2)}) copy-start(bf16[128,1536]{1,0:T(8,128)(2,1)} %param.27) | copy-start | bytes 1179652
  12.6 61.3 %copy-start.9 = (f32[2,512]{1,0:T(2,128)S(1)}, f32[2,512]{1,0:T(2,128)}, u32[]{:S(2)}) copy-start(f32[2,512]{1,0:T(2,128)} %param.25) | copy-start | bytes 12292
  12.6 48.8 %collective-permute-start = (bf16[512,2048]{1,0:T(8,128)(2,1)}, bf16[512,2048]{1,0:T(8,128)(2,1)S(1)}, u32[]{:S(2)}, u32[]{:S(2)}) collective-permute-start(bf16[512,2048]{1,0:T(8,128)(2,1)} %fusion.2.own_ref), channel_id=1, source_target_pairs={{0,1},{1,0},{2,3},{3,2},{4,5},{5,4},{6,7},{7,6},{8,9},{9,8},{10,11... | collective-permute-start | bytes 6291464 | tf_op jit(solution)/shard_map/ppermute | solution.py:310
  61.4 15.9 %copy-start.10 = (bf16[512,2048]{1,0:T(8,128)(2,1)}, bf16[512,2048]{1,0:T(8,128)(2,1)S(1)}, u32[]{:S(2)}) copy-start(bf16[512,2048]{1,0:T(8,128)(2,1)S(1)} %collective-permute-done.other_ref) | copy-start | bytes 6291460
  75.7 31.1 %collective-permute-start.1 = (bf16[1024,512]{1,0:T(8,128)(2,1)S(1)}, bf16[1024,512]{1,0:T(8,128)(2,1)S(1)}, u32[]{:S(2)}, u32[]{:S(2)}) collective-permute-start(bf16[1024,512]{1,0:T(8,128)(2,1)S(1)} %constant_dynamic-slice_fusion), channel_id=1, source_target_pairs={{0,1},{1,0},{2,3},{3,2},{4,5},{5,4},{6,7},{7,6},{8,9},{9,8},{10,11... | collective-permute-start | bytes 3145736 | tf_op jit(solution)/shard_map/ppermute | solution.py:328
  106.9 3.1 %collective-permute-start.3 = (bf16[1024,512]{1,0:T(8,128)(2,1)S(1)}, bf16[1024,512]{1,0:T(8,128)(2,1)S(1)}, u32[]{:S(2)}, u32[]{:S(2)}) collective-permute-start(bf16[1024,512]{1,0:T(8,128)(2,1)S(1)} %collective-permute-done.1), channel_id=1, source_target_pairs={{0,2},{2,0},{4,6},{6,4},{8,10},{10,8},{12,14},{14,12},{16,18},{18,... | collective-permute-start | bytes 3145736 | tf_op jit(solution)/shard_map/ppermute | solution.py:336
  107.0 14.5 %collective-permute-start.2 = (bf16[512,512]{1,0:T(8,128)(2,1)}, bf16[512,512]{1,0:T(8,128)(2,1)S(1)}, u32[]{:S(2)}, u32[]{:S(2)}) collective-permute-start(bf16[512,512]{1,0:T(8,128)(2,1)} %get-tuple-element.18), channel_id=1, source_target_pairs={{0,1},{1,0},{2,3},{3,2},{4,5},{5,4},{6,7},{7,6},{8,9},{9,8},{10,11... | collective-permute-start | bytes 1572872 | tf_op jit(solution)/shard_map/ppermute | solution.py:332
  121.5 0.8 copy-start.11
  132.0 26.1 %collective-permute-start.6 = (bf16[256,2048]{1,0:T(8,128)(2,1)S(1)}, bf16[256,2048]{1,0:T(8,128)(2,1)S(1)}, u32[]{:S(2)}, u32[]{:S(2)}) collective-permute-start(bf16[256,2048]{1,0:T(8,128)(2,1)S(1)} %get-tuple-element.23), channel_id=1, source_target_pairs={{0,1},{1,0},{2,3},{3,2},{4,5},{5,4},{6,7},{7,6},{8,9},{9,8},{10,11... | collective-permute-start | bytes 3145736 | tf_op jit(solution)/shard_map/ppermute | solution.py:348
  132.6 53.7 %collective-permute-start.4 = (bf16[256,2048]{1,0:T(8,128)(2,1)S(1)}, bf16[256,2048]{1,0:T(8,128)(2,1)S(1)}, u32[]{:S(2)}, u32[]{:S(2)}) collective-permute-start(bf16[256,2048]{1,0:T(8,128)(2,1)S(1)} %get-tuple-element.24), channel_id=1, source_target_pairs={{0,1},{1,0},{2,3},{3,2},{4,5},{5,4},{6,7},{7,6},{8,9},{9,8},{10,11... | collective-permute-start | bytes 3145736 | tf_op jit(solution)/shard_map/ppermute | solution.py:348
  158.1 14.9 %copy-start.2 = (bf16[256,2048]{1,0:T(8,128)(2,1)}, bf16[256,2048]{1,0:T(8,128)(2,1)S(1)}, u32[]{:S(2)}) copy-start(bf16[256,2048]{1,0:T(8,128)(2,1)S(1)} %collective-permute-done.6.x_ref) | copy-start | bytes 3145732
  184.9 31.9 %collective-permute-start.7 = (bf16[256,2048]{1,0:T(8,128)(2,1)}, bf16[256,2048]{1,0:T(8,128)(2,1)S(1)}, u32[]{:S(2)}, u32[]{:S(2)}) collective-permute-start(bf16[256,2048]{1,0:T(8,128)(2,1)} %ffn.5), channel_id=1, source_target_pairs={{0,1},{1,0},{2,3},{3,2},{4,5},{5,4},{6,7},{7,6},{8,9},{9,8},{10,11... | collective-permute-start | bytes 3145736 | tf_op jit(solution)/shard_map/ppermute | solution.py:353
  186.4 1.0 copy-start.1
  199.2 33.7 %collective-permute-start.5 = (bf16[256,2048]{1,0:T(8,128)(2,1)}, bf16[256,2048]{1,0:T(8,128)(2,1)S(1)}, u32[]{:S(2)}, u32[]{:S(2)}) collective-permute-start(bf16[256,2048]{1,0:T(8,128)(2,1)} %ffn.4), channel_id=1, source_target_pairs={{0,1},{1,0},{2,3},{3,2},{4,5},{5,4},{6,7},{7,6},{8,9},{9,8},{10,11... | collective-permute-start | bytes 3145736 | tf_op jit(solution)/shard_map/ppermute | solution.py:353
  216.8 1.0 copy-start.3
  232.9 1.0 copy-start.4
Sparse Core Ops, SparseCore 0:
  9.6 64.1 all-gather.2
  75.4 97.5 all-gather.4
